TPU v7x, 32 devices: a whole 2x2x4 slice. The times are simulated.
32 devices in a mesh: ep: 16 (over z, y, x), tp: 2 (over core).
Axes of the slice: x: 2, y: 2, z: 4, core: 2. Of those that a mesh axis runs over, the one named last changes fastest.
Arguments:
- tokens: bfloat16 [512, 2048], P('ep'), may hold values from -6 to 6
- lengths: int32 [512], P('ep'), may hold values from 128 to 1024
- key_cache: bfloat16 [512, 1024, 256], P('ep', None, 'tp'), may hold values from -1000 to 1000
- value_cache: bfloat16 [512, 1024, 256], P('ep', None, 'tp'), may hold values from -6 to 6
- gate_cache: float32 [512, 16, 1024], P('ep', 'tp'), may hold values from -130 to 0, as said below
- mix_gain: float32 [2048], replicated, may hold values from 0.1 to 1.9
- query_weight: bfloat16 [2048, 1024], P(None, 'tp'), may hold values from -0.125 to 0.125
- key_weight: bfloat16 [2048, 256], P(None, 'tp'), may hold values from -0.125 to 0.125
- value_weight: bfloat16 [2048, 256], P(None, 'tp'), may hold values from -0.125 to 0.125
- forget_weight: bfloat16 [2048, 16], P(None, 'tp'), may hold values from -0.125 to 0.125
- out_weight: bfloat16 [1024, 2048], P('tp'), may hold values from -0.1875 to 0.1875
- expert_gain: float32 [2048], replicated, may hold values from 0.1 to 1.9
- routes: int32 [512, 2], P('ep'), may hold values from 0 to 7, all different within a row; in each aligned block of 32 rows (0 to 31, 32 to 63, ...) at most 12 rows name the same one
- route_weights: float32 [512, 2], P('ep'), may hold values from 0.2 to 1
- expert_gate: bfloat16 [2048, 65536], P(None, ('ep', 'tp')), may hold values from -0.125 to 0.125
- expert_up: bfloat16 [2048, 65536], P(None, ('ep', 'tp')), may hold values from -0.125 to 0.125
- expert_down: bfloat16 [65536, 2048], P(('ep', 'tp')), may hold values from -0.0625 to 0.0625
Outputs:
- layer_out: bfloat16 [512, 2048], P('ep')
Inputs may be any that keep to these rules, and one draw needn't show every extreme that they name: `routes`: within the rows of one index of ep, no expert is named more than 12 times, and in every draw some expert is named exactly 12 times in some such rows; the 2 experts of a row differ. `gate_cache`: for each sequence and head the values never rise along the cache positions.
All inputs are finite; a program needn't handle non-finite values.
Results may differ from a plain program's by a relative error of at most 0.013.
Values may be sent and summed in bfloat16 or wider, within the bound.
No kernel may reach another device: no remote copies, remote signals or barrier semaphores. Data moves between devices by JAX's collectives and lax.ppermute only.
A program may use at most 128 MiB of HBM per device.

v0:
```python
import jax
import jax.numpy as jnp
from jax import lax
from jax.sharding import PartitionSpec as P

HD = 64
EXPERTS = 8
CAP = 12


eps = 1e-06


def normed(values, gain):
    floats = values.astype(jnp.float32)
    return floats * lax.rsqrt(jnp.mean(floats * floats, axis=-1, keepdims=True) + eps) * gain


def attend(queries, key_new, value_new, log_gate, key_rows, value_rows, cumulative, length):
    seq_count, head_count, head_size = queries.shape
    kv_count = key_new.shape[1]
    group_size = head_count // kv_count
    cache_locations = key_rows.shape[1]
    factor = head_size ** (-0.5)
    grouped = queries.reshape(seq_count, kv_count, group_size, head_size)
    key_split = key_rows.reshape(seq_count, cache_locations, kv_count, head_size)
    value_split = value_rows.reshape(seq_count, cache_locations, kv_count, head_size)
    scores = (
        jnp.einsum(
            "skgd,spkd->skgp", grouped, key_split, preferred_element_type=jnp.float32
        ).reshape(seq_count, head_count, cache_locations)
        * factor
    )
    positions = jnp.arange(cache_locations, dtype=jnp.int32)
    latest = jnp.sum(
        jnp.where(positions[None, None, :] == (length - 1)[:, None, None], cumulative, 0.0), axis=-1
    )
    scores = scores + (latest + log_gate)[..., None] - cumulative
    valid = positions[None, None, :] < length[:, None, None]
    scores = jnp.where(valid, scores, -jnp.inf)
    own_score = (
        jnp.einsum("skgd,skd->skg", grouped, key_new, preferred_element_type=jnp.float32).reshape(
            seq_count, head_count
        )
        * factor
    )
    highest = jnp.maximum(jnp.max(scores, axis=-1), own_score)
    raised = jnp.exp(scores - highest[..., None])
    own_raised = jnp.exp(own_score - highest)
    denominator = jnp.sum(raised, axis=-1) + own_raised
    weights = (raised / denominator[..., None]).astype(jnp.bfloat16)
    own_weight = (own_raised / denominator).astype(jnp.bfloat16)
    mixed = jnp.einsum(
        "skgp,spkd->skgd",
        weights.reshape(seq_count, kv_count, group_size, cache_locations),
        value_split,
        preferred_element_type=jnp.float32,
    )
    mixed = (
        mixed
        + own_weight.reshape(seq_count, kv_count, group_size)[..., None].astype(jnp.float32)
        * value_new.astype(jnp.float32)[:, :, None, :]
    )
    return mixed.reshape(seq_count, head_count * head_size).astype(jnp.bfloat16)


def expert_work(rows_in, expert_gate, expert_up, expert_down):
    leading = rows_in.shape[:-1]
    flat_rows = rows_in.reshape(-1, rows_in.shape[-1])
    gate_out = jnp.dot(flat_rows, expert_gate, preferred_element_type=jnp.float32)
    up_out = jnp.dot(flat_rows, expert_up, preferred_element_type=jnp.float32)
    hidden = (jax.nn.silu(gate_out) * up_out).astype(jnp.bfloat16)
    return jnp.dot(hidden, expert_down, preferred_element_type=jnp.float32).reshape(
        leading + (expert_down.shape[1],)
    )


def combine(returned, target, route_weights):
    capacity = returned.shape[1]
    columns = returned.shape[2]
    blocks = jnp.sum(
        returned.reshape(EXPERTS, -1, capacity, columns).astype(jnp.float32), axis=1
    ).reshape(EXPERTS * capacity, columns)
    picked = jnp.take(blocks, target, axis=0).reshape(route_weights.shape + (columns,))
    return jnp.sum(picked * route_weights[..., None], axis=1)


def on_device(
    tokens,
    lengths,
    key_cache,
    value_cache,
    gate_cache,
    mix_gain,
    query_weight,
    key_weight,
    value_weight,
    forget_weight,
    out_weight,
    expert_gain,
    routes,
    route_weights,
    expert_gate,
    expert_up,
    expert_down,
):
    seq_count = tokens.shape[0]
    width = tokens.shape[1]
    normal_in = normed(tokens, mix_gain).astype(jnp.bfloat16)
    queries = (
        jnp.dot(normal_in, query_weight, preferred_element_type=jnp.float32)
        .astype(jnp.bfloat16)
        .reshape(seq_count, -1, HD)
    )
    key_new = (
        jnp.dot(normal_in, key_weight, preferred_element_type=jnp.float32)
        .astype(jnp.bfloat16)
        .reshape(seq_count, -1, HD)
    )
    value_new = (
        jnp.dot(normal_in, value_weight, preferred_element_type=jnp.float32)
        .astype(jnp.bfloat16)
        .reshape(seq_count, -1, HD)
    )
    log_gate = jax.nn.log_sigmoid(
        jnp.dot(normal_in, forget_weight, preferred_element_type=jnp.float32)
    )
    mixed = attend(
        queries, key_new, value_new, log_gate, key_cache, value_cache, gate_cache, lengths
    )
    partial_out = jnp.dot(mixed, out_weight, preferred_element_type=jnp.float32).astype(
        jnp.bfloat16
    )
    residual = (
        tokens.astype(jnp.float32) + lax.psum(partial_out, "tp").astype(jnp.float32)
    ).astype(jnp.bfloat16)
    expert_in = normed(residual, expert_gain).astype(jnp.bfloat16)
    top_count = routes.shape[1]
    flat_routes = routes.reshape(-1)
    one_hot = (flat_routes[:, None] == jnp.arange(EXPERTS, dtype=jnp.int32)[None, :]).astype(
        jnp.int32
    )
    slot_index = jnp.sum((jnp.cumsum(one_hot, axis=0) - 1) * one_hot, axis=1)
    target = flat_routes * CAP + slot_index
    dispatch = (jnp.arange(EXPERTS * CAP, dtype=jnp.int32)[:, None] == target[None, :]).astype(
        jnp.bfloat16
    )
    repeated = jnp.repeat(expert_in, top_count, axis=0)
    outgoing = jnp.dot(dispatch, repeated, preferred_element_type=jnp.float32).astype(jnp.bfloat16)
    pieces = lax.axis_size("ep") // EXPERTS
    outgoing = jnp.broadcast_to(
        outgoing.reshape(EXPERTS, 1, CAP, width), (EXPERTS, pieces, CAP, width)
    ).reshape(EXPERTS * pieces, CAP, width)
    half_width = width // lax.axis_size("tp")
    start = lax.axis_index("tp") * half_width
    outgoing_half = lax.dynamic_slice_in_dim(outgoing, start, half_width, 2)
    full_rows = lax.all_gather(
        lax.all_to_all(outgoing_half, "ep", split_axis=0, concat_axis=0, tiled=True),
        "tp",
        axis=2,
        tiled=True,
    )
    partial_rows = expert_work(full_rows, expert_gate, expert_up, expert_down).astype(jnp.bfloat16)
    share = (
        lax.psum_scatter(partial_rows, "tp", scatter_dimension=2, tiled=True)
        .astype(jnp.float32)
        .astype(jnp.bfloat16)
    )
    returned = lax.all_to_all(share, "ep", split_axis=0, concat_axis=0, tiled=True)
    mixture = combine(returned, target, route_weights)
    own_half = lax.dynamic_slice_in_dim(residual, start, half_width, 1).astype(jnp.float32)
    return lax.all_gather((own_half + mixture).astype(jnp.bfloat16), "tp", axis=1, tiled=True)


def solution(mesh):
    return jax.shard_map(
        on_device,
        mesh=mesh,
        in_specs=(
            P("ep", None),
            P("ep"),
            P("ep", None, "tp"),
            P("ep", None, "tp"),
            P("ep", "tp", None),
            P(),
            P(None, "tp"),
            P(None, "tp"),
            P(None, "tp"),
            P(None, "tp"),
            P("tp", None),
            P(),
            P("ep", None),
            P("ep", None),
            P(None, ("ep", "tp")),
            P(None, ("ep", "tp")),
            P(("ep", "tp"), None),
        ),
        out_specs=P("ep", None),
        check_vma=False,
    )
```

profile of v0, /device:TPU:0, one launch (start us, length us, event | category | flops | bytes accessed | tf_op | source)
XLA Modules:
  0.0 167.7 jit_solution(255999665573253015)
XLA Ops:
  6.5 0.8 broadcast_add_fusion
  7.3 0.7 iota_compare_fusion.1
  8.1 1.0 fusion.7
  9.1 2.2 %convolution_convert_fusion.3 = bf16[32,512]{1,0:T(8,128)(2,1)S(1)} fusion(bf16[2048,512]{1,0:T(8,128)(2,1)} %param.23, bf16[32,2048]{1,0:T(8,128)(2,1)} %param.17, f32[2048]{0:T(1024)} %param.22, f32[32]{0:T(128)S(1)} %add_rsqrt_fusion.1), kind=kOutput, calls=%fused_computation.9 | convolution fusion | flops 67387392 | bytes 2269312 | tf_op jit(solution)/shard_map/dot_general | solution.py:111
  11.5 11.9 %copy.45 = bf16[32,1024,128]{1,2,0:T(8,128)(2,1)} copy(bf16[32,1024,128]{2,1,0:T(8,128)(2,1)} %param.19) | data formatting | bytes 16777216 | tf_op args[2]
  23.4 4.6 %convolution_multiply_fusion.1 = f32[32,2,4,1024]{3,2,1,0:T(4,128)S(1)} fusion(bf16[32,2,4,64]{3,2,1,0:T(4,128)(2,1)S(1)} %reshape_reshape.3, bf16[32,1024,2,64]{1,3,2,0:T(8,128)(2,1)} %bitcast.37), kind=kOutput, calls=%fused_computation.6 | convolution fusion | flops 33816576 | bytes 9469952 | tf_op jit(solution)/shard_map/skgd,spkd->skgp/dot_general | solution.py:29
  28.0 1.4 mul.132
  29.5 1.5 select_reduce_fusion
  31.3 1.9 %fusion.25 = (f32[32,8]{1,0:T(8,128)S(1)}, f32[32,8,1024]{2,1,0:T(8,128)S(1)}) fusion(f32[32,8,1024]{2,1,0:T(8,128)} %param.21, f32[32,8,1024]{2,1,0:T(8,128)} %mul.132, f32[32,8]{1,0:T(8,128)S(1)} %copy.47, pred[32,1024]{1,0:T(8,128)(4,1)S(1)} %iota_compare_fusion.1), kind=kLoop, calls=%fused_computation.64 | loop fusion | flops 1048320 | bytes 3180544 | tf_op jit(solution)/shard_map/reduce_max | solution.py:47
  33.3 1.3 convolution_convert_fusion.5
  35.5 1.1 divide_convert_fusion
  36.6 1.2 reshape.188
  38.0 1.3 fusion.2
  39.4 11.9 %copy.52 = bf16[32,1024,128]{1,2,0:T(8,128)(2,1)} copy(bf16[32,1024,128]{2,1,0:T(8,128)(2,1)} %param.20) | data formatting | bytes 16777216 | tf_op args[3]
  51.3 5.7 %fusion.1 = bf16[32,2,4,64]{3,2,1,0:T(4,128)(2,1)S(1)} fusion(bf16[32,2,4,1024]{3,2,1,0:T(4,128)(2,1)S(1)} %reshape.188, bf16[32,1024,2,64]{1,3,2,0:T(8,128)(2,1)} %bitcast.38, f32[32,2,64]{2,1,0:T(2,128)S(1)} %reshape.195, f32[32,2,4]{2,1,0:T(2,128)S(1)} %copy.55), kind=kOutput, calls=%fused_computation.8 | convolution fusion | flops 33603584 | bytes 8963072 | tf_op jit(solution)/shard_map/skgp,spkd->skgd/dot_general | solution.py:53
  57.1 1.1 convolution_convert_fusion.2
  58.9 20.2 %all-reduce.2.cloned.1.call-done = bf16[32,2048]{1,0:T(8,128)(2,1)} async-done(((bf16[32,2048]{1,0:T(8,128)(2,1)}), bf16[32,2048]{1,0:T(8,128)(2,1)}) %all-reduce.2.cloned.1.call-update) | async-done | bytes 131088 | tf_op jit(solution)/shard_map/psum | solution.py:135
  79.1 1.1 fusion.4
  81.6 22.1 %all_to_all.10 = bf16[16,12,1024]{2,1,0:T(8,128)(2,1)S(1)} all-to-all(bf16[16,12,1024]{2,1,0:T(8,128)(2,1)S(1)} %constant_dynamic-slice_fusion), channel_id=1, replica_groups=mesh['ep'=16,'tp'=2] {'ep'}, dimensions={0} | all-to-all | bytes 786432 | tf_op jit(solution)/shard_map/all_to_all | solution.py:158
  103.7 2.7 %all_gather.6 = bf16[16,12,2048]{2,1,0:T(8,128)(2,1)S(1)} all-gather(bf16[16,12,1024]{2,1,0:T(8,128)(2,1)S(1)} %all_to_all.10), channel_id=1, replica_groups=mesh['ep'=16,'tp'=2] {'tp'}, dimensions={2}, use_global_device_ids=true | all-gather | bytes 1179648 | tf_op jit(solution)/shard_map/all_gather | solution.py:157
  106.6 6.3 %fusion.27 = f32[192,2048]{1,0:T(8,128)} fusion(bf16[192,2048]{1,0:T(8,128)(2,1)S(1)} %reshape.193, bf16[2048,2048]{1,0:T(8,128)(2,1)} %param.31), kind=kOutput, calls=%fused_computation.66 | convolution fusion | flops 1610612736 | bytes 10747904 | tf_op jit(solution)/shard_map/dot_general | solution.py:70
  113.0 10.9 %convolution_convert_fusion = bf16[192,2048]{1,0:T(8,128)(2,1)} fusion(bf16[2048,2048]{1,0:T(8,128)(2,1)} %param.33, bf16[192,2048]{1,0:T(8,128)(2,1)S(1)} %reshape.193, bf16[2048,2048]{1,0:T(8,128)(2,1)} %param.32, f32[192,2048]{1,0:T(8,128)} %fusion.27), kind=kOutput, calls=%fused_computation.2 | convolution fusion | flops 3223977984 | bytes 19922944 | tf_op jit(solution)/shard_map/dot_general | solution.py:73
  123.8 2.1 %convert_element_type.110 = bf16[16,12,2048]{2,1,0:T(8,128)(2,1)} reshape(bf16[192,2048]{1,0:T(8,128)(2,1)} %convolution_convert_fusion) | data formatting | bytes 1572864 | tf_op jit(solution)/shard_map/convert_element_type | solution.py:163
  126.1 6.8 %reduce-scatter.2.cloned.1.call-done = bf16[16,12,1024]{2,1,0:T(8,128)(2,1)} async-done(((bf16[16,12,2048]{2,1,0:T(8,128)(2,1)}), bf16[16,12,1024]{2,1,0:T(8,128)(2,1)}) %reduce-scatter.2.cloned.1.call-update) | async-done | bytes 393232 | tf_op jit(solution)/shard_map/reduce_scatter | solution.py:165
  132.9 6.8 %all-to-all-start.1 = ((bf16[16,12,1024]{2,1,0:T(8,128)(2,1)}), bf16[16,12,1024]{2,1,0:T(8,128)(2,1)S(1)}, u32[]{:S(2)}, u32[]{:S(2)}) async-start(bf16[16,12,1024]{2,1,0:T(8,128)(2,1)} %reduce-scatter.2.cloned.1.call-done), calls=%async_computation.2 | async-start | bytes 1048576 | tf_op jit(solution)/shard_map/all_to_all | solution.py:169
  140.0 0.7 copy.58
  141.3 13.8 %all-to-all-done.1 = bf16[16,12,1024]{2,1,0:T(8,128)(2,1)S(1)} async-done(((bf16[16,12,1024]{2,1,0:T(8,128)(2,1)}), bf16[16,12,1024]{2,1,0:T(8,128)(2,1)S(1)}, u32[]{:S(2)}, u32[]{:S(2)}) %all-to-all-start.1) | async-done | bytes 393248 | tf_op jit(solution)/shard_map/all_to_all | solution.py:169
  155.3 0.8 gather_fusion
  156.3 1.2 multiply_reduce_fusion
  157.4 0.9 add_convert_fusion
  158.3 1.9 %all_gather.7 = bf16[32,2048]{1,0:T(8,128)(2,1)S(1)} all-gather(bf16[32,1024]{1,0:T(8,128)(2,1)S(1)} %add_convert_fusion), channel_id=1, replica_groups=mesh['ep'=16,'tp'=2] {'tp'}, dimensions={1}, use_global_device_ids=true | all-gather | bytes 196608 | tf_op jit(solution)/shard_map/all_gather | solution.py:172
  160.2 0.7 copy.65
  (70 shorter events, 5.5 us)
Async XLA Ops:
  6.5 50.6 %copy-start = (bf16[512,2048]{1,0:T(8,128)(2,1)S(1)}, bf16[512,2048]{1,0:T(8,128)(2,1)}, u32[]{:S(2)}) copy-start(bf16[512,2048]{1,0:T(8,128)(2,1)} %param.27) | copy-start | bytes 6291460
  6.5 72.6 %all-reduce.2.cloned.1.call-start = ((), (), s32[]{:S(2)}) async-start(), calls=%async_computation.3 | async-start | bytes 262144 | tf_op jit(solution)/shard_map/psum | solution.py:135
  23.4 7.6 %copy-start.2 = (bf16[32,2048]{1,0:T(8,128)(2,1)S(1)}, bf16[32,2048]{1,0:T(8,128)(2,1)}, u32[]{:S(2)}) copy-start(bf16[32,2048]{1,0:T(8,128)(2,1)} %param.17) | copy-start | bytes 393220
  23.4 7.6 %copy-start.4 = (f32[2048]{0:T(1024)S(1)}, f32[2048]{0:T(1024)}, u32[]{:S(2)}) copy-start(f32[2048]{0:T(1024)} %param.22) | copy-start | bytes 24580
  23.4 7.6 %copy-start.8 = (bf16[2048,8]{0,1:T(8,128)(2,1)S(1)}, bf16[2048,8]{0,1:T(8,128)(2,1)}, u32[]{:S(2)}) copy-start(bf16[2048,8]{0,1:T(8,128)(2,1)} %param.26) | copy-start | bytes 98308
  51.3 7.0 %copy-start.5 = (s32[32,2]{0,1:T(2,128)S(1)}, s32[32,2]{0,1:T(2,128)}, u32[]{:S(2)}) copy-start(s32[32,2]{0,1:T(2,128)} %param.29) | copy-start | bytes 772
  51.3 28.9 %copy-start.6 = (f32[2048]{0:T(1024)S(1)}, f32[2048]{0:T(1024)}, u32[]{:S(2)}) copy-start(f32[2048]{0:T(1024)} %param.28) | copy-start | bytes 24580
  58.3 74.6 %reduce-scatter.2.cloned.1.call-start = ((), (), s32[]{:S(2)}) async-start(), calls=%async_computation.4 | async-start | bytes 1572864 | tf_op jit(solution)/shard_map/reduce_scatter | solution.py:165
  80.2 0.7 copy-start.3
  113.0 27.7 %copy-start.7 = (f32[32,2]{0,1:T(2,128)S(1)}, f32[32,2]{0,1:T(2,128)}, u32[]{:S(2)}) copy-start(f32[32,2]{0,1:T(2,128)} %param.30) | copy-start | bytes 772
  113.0 47.9 %copy-start.1 = (bf16[512,2048]{1,0:T(8,128)(2,1)S(1)}, bf16[512,2048]{1,0:T(8,128)(2,1)}, u32[]{:S(2)}) copy-start(bf16[512,2048]{1,0:T(8,128)(2,1)} %param.27) | copy-start | bytes 6291460
  132.9 22.3 %all-to-all-start.1 = ((bf16[16,12,1024]{2,1,0:T(8,128)(2,1)}), bf16[16,12,1024]{2,1,0:T(8,128)(2,1)S(1)}, u32[]{:S(2)}, u32[]{:S(2)}) async-start(bf16[16,12,1024]{2,1,0:T(8,128)(2,1)} %reduce-scatter.2.cloned.1.call-done), calls=%async_computation.2 | async-start | bytes 1048576 | tf_op jit(solution)/shard_map/all_to_all | solution.py:169
Sparse Core Ops, SparseCore 0:
  58.4 20.6 all-reduce.1
  126.1 6.7 reduce-scatter.1
where the time goes:
time: 169 us; the launch traced here: 168 us
  waiting for transfers between devices  40.8 us (24%)
  matrix products  34.1 us (20%)
  local copies, waits for them, and re-layouts  33.9 us (20%)
  blocking collectives  26.7 us (16%)
  between operations  13.7 us (8%)
  other arithmetic  11.7 us (7%)
  starting transfers between devices  6.82 us (4%)
    unnamed x23, local copies, waits for them, and re-layouts  25.3 us
    all_to_all x1, blocking collectives, on_device(): lax.all_to_all(outgoing_half, 'ep', split_axis=0, concat_axis=0, tiled=True)  22.1 us
    psum x1, waiting for transfers between devices, on_device(): lax.psum(partial_out, 'tp').astype(jnp.float32)  20.2 us
    all_to_all x1, waiting for transfers between devices, on_device(): lax.all_to_all(share, 'ep', split_axis=0, concat_axis=0, tiled=True)  13.8 us
    dot_general x1, matrix products, expert_work(): jnp.dot(hidden, expert_down, preferred_element_type=jnp.float32)  10.9 us
    all_to_all x1, starting transfers between devices, on_device(): lax.all_to_all(share, 'ep', split_axis=0, concat_axis=0, tiled=True)  6.78 us
    reduce_scatter x1, waiting for transfers between devices, on_device(): lax.psum_scatter(partial_rows, 'tp', scatter_dimension=2, tiled=True)  6.77 us
    dot_general x1, matrix products, expert_work(): jnp.dot(flat_rows, expert_gate, preferred_element_type=jnp.float32)  6.34 us
  transfers between devices with their start and end apart: 3, of which 3 were waited for; matrix products, arithmetic and copies ran while one was open for 1% of the time, Pallas kernels for 0%

commit v1 on v0

v1 whole, which is shorter than its diff:
```python
import functools

import jax
import jax.numpy as jnp
from jax import lax
from jax.experimental import pallas as pl
from jax.experimental.pallas import tpu as pltpu
from jax.sharding import PartitionSpec as P

HD = 64
EXPERTS = 8
CAP = 12
LANES = 128
GROUP = 8
STEP = 128

eps = 1e-06
f32 = jnp.float32
bf16 = jnp.bfloat16
VMEM_SPEC = pl.BlockSpec(memory_space=pltpu.VMEM)
HBM_SPEC = pl.BlockSpec(memory_space=pltpu.HBM)
NT = (((1,), (1,)), ((), ()))
TN = (((0,), (0,)), ((), ()))


def in_hbm(array):
    return pltpu.with_memory_space_constraint(array, pltpu.HBM)


def in_vmem(array):
    return pltpu.with_memory_space_constraint(array, pltpu.VMEM)


def iota(shape, dim):
    return lax.broadcasted_iota(jnp.int32, shape, dim)


def quotient(values, divisor):
    return jnp.floor((values.astype(f32) + 0.5) * (1.0 / divisor))


def normed(values, gain):
    floats = values.astype(f32)
    return floats * lax.rsqrt(jnp.mean(floats * floats, axis=-1, keepdims=True) + eps) * gain


def slot_matrix(routes, rows, pieces):
    count = routes.shape[1]
    first, second = routes[0:1, :], routes[1:2, :]
    expert = iota((EXPERTS, count), 0)
    named = ((first == expert) | (second == expert)).astype(f32).astype(bf16)
    earlier = (iota((count, count), 0) < iota((count, count), 1)).astype(f32).astype(bf16)
    slot = jnp.dot(named, earlier, preferred_element_type=f32) + (expert * CAP).astype(f32)
    place0 = jnp.sum(jnp.where(first == expert, slot, 0.0), axis=0, keepdims=True)
    place1 = jnp.sum(jnp.where(second == expert, slot, 0.0), axis=0, keepdims=True)
    unused = jnp.full((1, 2 * count), -1.0, f32)
    lower = jnp.concatenate([place0, place1, unused], axis=1)
    upper = jnp.concatenate([unused, place0, place1], axis=1)
    row = iota((rows, 4 * count), 0)
    block = quotient(row, 2 * CAP)
    within = row.astype(f32) - block * (2 * CAP)
    half = within >= CAP
    wanted = quotient(block, pieces) * CAP + jnp.where(half, within - CAP, within)
    hit = jnp.where(half, (wanted == upper).astype(f32), (wanted == lower).astype(f32))
    return hit.astype(bf16)


def attention_kernel(
    pieces,
    lengths_in,
    tokens,
    gain,
    forget,
    routes,
    wq,
    wk,
    wv,
    wo,
    keys,
    values,
    gates,
    partial_out,
    slots,
    lengths_s,
    tokens_v,
    gain_v,
    forget_v,
    routes_v,
    wq_v,
    wk_v,
    wv_v,
    wo_v,
    keys_v,
    values_v,
    gates_v,
    query_v,
    key_new_v,
    value_new_v,
    log_gate_v,
    mixed_v,
    small_sem,
    weight_sem,
    gate_sem,
    key_sem,
    value_sem,
):
    seq_count, positions, _ = keys.shape
    heads = gates.shape[1]
    pairs = heads // 2
    groups = seq_count // GROUP

    lengths = lengths_s
    small = [
        pltpu.make_async_copy(src, dst, small_sem.at[i])
        for i, (src, dst) in enumerate(
            (
                (lengths_in, lengths_s),
                (routes, routes_v),
                (tokens, tokens_v),
                (gain, gain_v),
                (forget, forget_v),
            )
        )
    ]
    copies = [
        pltpu.make_async_copy(src, dst, weight_sem.at[i])
        for i, (src, dst) in enumerate(((wq, wq_v), (wk, wk_v), (wv, wv_v), (wo, wo_v)))
    ]

    def used(s):
        return pl.multiple_of((lengths[s] + STEP - 1) // STEP * STEP, STEP)

    def key_copy(s):
        window = pl.ds(0, used(s))
        return pltpu.make_async_copy(keys.at[s, window], keys_v.at[s, window], key_sem.at[s])

    def value_copy(s):
        window = pl.ds(0, used(s))
        return pltpu.make_async_copy(values.at[s, window], values_v.at[s, window], value_sem.at[s])

    def gate_copy(g):
        window = pl.ds(g * GROUP, GROUP)
        return pltpu.make_async_copy(gates.at[window], gates_v.at[window], gate_sem.at[g])

    for c in small + copies[:3]:
        c.start()

    def start_keys(g):
        gate_copy(g).start()
        for j in range(GROUP):
            key_copy(g * GROUP + j).start()

    def start_values(g):
        for j in range(GROUP):
            value_copy(g * GROUP + j).start()

    small[0].wait()
    start_keys(0)

    def clear(s, _):
        values_v[s] = jnp.zeros(values_v.shape[1:], bf16)
        return 0

    lax.fori_loop(0, seq_count, clear, 0)
    start_values(0)

    def start_rest(g, _):
        start_keys(g)
        start_values(g)
        return 0

    lax.fori_loop(1, groups, start_rest, 0)
    copies[3].start()

    for c in small[1:]:
        c.wait()
    slots[...] = slot_matrix(routes_v[...], slots.shape[0], pieces)

    normal_in = normed(tokens_v[...], gain_v[...]).astype(bf16)
    gate_in = lax.dot_general(forget_v[...], normal_in, NT, preferred_element_type=f32)
    log_gate_v[:, :seq_count] = jnp.minimum(gate_in, 0.0) - jnp.log1p(jnp.exp(-jnp.abs(gate_in)))
    low = iota((seq_count, LANES), 1) < HD
    for c in copies[:3]:
        c.wait()
    query = jnp.dot(normal_in, wq_v[...], preferred_element_type=f32).astype(bf16).astype(f32)
    query = query * (HD**-0.5)
    key_new_v[...] = (
        jnp.dot(normal_in, wk_v[...], preferred_element_type=f32).astype(bf16).astype(f32)
    )
    value_new_v[...] = (
        jnp.dot(normal_in, wv_v[...], preferred_element_type=f32).astype(bf16).astype(f32)
    )
    for j in range(pairs):
        val = query[:, j * LANES : (j + 1) * LANES]
        turned = pltpu.roll(val, HD, 1)
        if j < pairs // 2:
            one, two = jnp.where(low, val, 0.0), jnp.where(low, turned, 0.0)
        else:
            one, two = jnp.where(low, 0.0, turned), jnp.where(low, 0.0, val)
        query_v[:, 2 * j, :] = one
        query_v[:, 2 * j + 1, :] = two

    lane = iota((heads, LANES), 1)
    position = iota((heads, positions), 1)

    def group_step(g, _):
        gate_copy(g).wait()
        scored = []
        for j in range(GROUP):
            s = g * GROUP + j
            key_copy(s).wait()
        for j in range(GROUP):
            s = g * GROUP + j
            length = lengths[s]
            query_s = query_v[s]
            score = lax.dot_general(
                query_s.astype(bf16), keys_v[s], NT, preferred_element_type=f32
            )
            last = length - 1
            start = pl.multiple_of(last // LANES * LANES, LANES)
            near = gates_v[s, :, pl.ds(start, LANES)]
            picked = jnp.where(lane == last - start, near, 0.0) + jnp.where(
                lane == s, log_gate_v[...], 0.0
            )
            offset = jnp.sum(picked, axis=1, keepdims=True)
            own = jnp.sum(query_s * key_new_v[pl.ds(s, 1), :], axis=1, keepdims=True)
            score = jnp.where(position < length, score + offset - gates_v[s], -jnp.inf)
            highest = jnp.maximum(jnp.max(score, axis=1, keepdims=True), own)
            raised = jnp.exp(score - highest)
            own_raised = jnp.exp(own - highest)
            total = jnp.sum(raised, axis=1, keepdims=True) + own_raised
            scored.append((raised.astype(bf16), own_raised, total))
        for j in range(GROUP):
            s = g * GROUP + j
            value_copy(s).wait()
        for j in range(GROUP):
            s = g * GROUP + j
            raised, own_raised, total = scored[j]
            product = jnp.dot(raised, values_v[s], preferred_element_type=f32)
            product = product + own_raised * value_new_v[pl.ds(s, 1), :]
            mixed_v[s] = product / total
        return 0

    lax.fori_loop(0, groups, group_step, 0)

    parts = []
    for j in range(pairs):
        one, two = mixed_v[:, 2 * j, :], mixed_v[:, 2 * j + 1, :]
        if j < pairs // 2:
            parts.append(jnp.where(low, one, pltpu.roll(two, HD, 1)))
        else:
            parts.append(jnp.where(low, pltpu.roll(one, HD, 1), two))
    mixed = jnp.concatenate(parts, axis=1).astype(bf16)
    copies[3].wait()
    partial_out[...] = jnp.dot(mixed, wo_v[...], preferred_element_type=f32).astype(bf16)


def dispatch_kernel(tokens, own, other, gain, slots, outgoing, own_half, normal_v, full_v):
    columns = own_half.shape[1]
    quarter = columns // 2
    residual = tokens[...].astype(f32) + own[...].astype(f32) + other[...].astype(f32)
    residual = residual.astype(bf16)
    full_v[...] = residual
    normal_v[...] = normed(residual, gain[...]).astype(bf16)
    start = pl.multiple_of(lax.axis_index("tp") * columns, columns)
    own_half[...] = full_v[:, pl.ds(start, columns)]
    first = normal_v[:, pl.ds(start, quarter)]
    second = normal_v[:, pl.ds(pl.multiple_of(start + quarter, quarter), quarter)]
    stacked = jnp.concatenate([first, first, second, second], axis=0)
    outgoing[...] = jnp.dot(slots[...], stacked, preferred_element_type=f32).astype(bf16)


def gather_matrix(rows_in, rows_out, half, turned):
    shape = (rows_in, rows_out) if turned else (rows_out, rows_in)
    dim = 1 if turned else 0
    row = iota(shape, dim)
    source = quotient(row, CAP)
    target = source * (2 * CAP) + half * CAP + (row.astype(f32) - source * CAP)
    return (target == iota(shape, 1 - dim).astype(f32)).astype(f32).astype(bf16)


def expert_kernel(
    parts,
    mine,
    others,
    w_gate,
    w_up,
    w_down,
    out_mine,
    out_others,
    rows_v,
    hidden_v,
    down_v,
    down_sem,
):
    width, units = w_gate.shape
    block = units // parts
    columns = width // 2
    quarter = columns // 2
    me = lax.axis_index("tp")

    def down_start(q):
        return pl.multiple_of(jnp.where(q < 2, 1 - me, me) * columns + (q % 2) * quarter, quarter)

    def down_copy(q):
        window = pl.ds(down_start(q), quarter)
        return pltpu.make_async_copy(w_down.at[:, window], down_v.at[q], down_sem.at[q])

    for q in range(4):
        down_copy(q).start()

    rows_in = mine.shape[0]
    rows_out = rows_in // 2
    span = min(rows_in, 16 * 2 * CAP)
    span_out = span // 2
    for half in range(2):
        matrix = gather_matrix(span, span_out, half, False)
        for piece in range(rows_in // span):
            taken = pl.ds(piece * span, span)
            given = pl.ds(piece * span_out, span_out)
            for source, side in ((mine, me), (others, 1 - me)):
                start = pl.multiple_of(side * columns + half * quarter, quarter)
                rows_v[given, pl.ds(start, quarter)] = jnp.dot(
                    matrix, source[taken, :], preferred_element_type=f32
                ).astype(bf16)

    for j in range(parts):
        window = slice(j * block, (j + 1) * block)
        gate_out = jnp.dot(rows_v[...], w_gate[:, window], preferred_element_type=f32)
        up_out = jnp.dot(rows_v[...], w_up[:, window], preferred_element_type=f32)
        hidden = gate_out * jax.nn.sigmoid(gate_out) * up_out
        hidden_v[:, j * block : (j + 1) * block] = hidden.astype(bf16)

    spread = [gather_matrix(span, span_out, half, True) for half in range(2)]
    for side, target in ((0, out_others), (1, out_mine)):
        results = []
        for half in range(2):
            q = 2 * side + half
            down_copy(q).wait()
            results.append(
                jnp.dot(hidden_v[...], down_v[q], preferred_element_type=f32).astype(bf16)
            )
        for piece in range(rows_in // span):
            taken = slice(piece * span_out, (piece + 1) * span_out)
            target[pl.ds(piece * span, span), :] = (
                jnp.dot(spread[0], results[0][taken], preferred_element_type=f32)
                + jnp.dot(spread[1], results[1][taken], preferred_element_type=f32)
            ).astype(bf16)


def combine_kernel(returned, slots, own_half, route_weights, out):
    seq_count = own_half.shape[0]
    quarter = returned.shape[1]
    picked = lax.dot_general(slots[...], returned[...], TN, preferred_element_type=f32)
    square = iota((seq_count, seq_count), 0) == iota((seq_count, seq_count), 1)
    weights = [
        jnp.sum(jnp.where(square, route_weights[k : k + 1, :], 0.0), axis=1, keepdims=True)
        for k in range(2)
    ]
    for half in range(2):
        base = half * 2 * seq_count
        mixture = picked[base : base + seq_count] * weights[0]
        mixture = mixture + picked[base + seq_count : base + 2 * seq_count] * weights[1]
        span = slice(half * quarter, (half + 1) * quarter)
        out[:, span] = (own_half[:, span].astype(f32) + mixture).astype(bf16)


def on_device(
    tokens,
    lengths,
    key_cache,
    value_cache,
    gate_cache,
    mix_gain,
    query_weight,
    key_weight,
    value_weight,
    forget_weight,
    out_weight,
    expert_gain,
    routes,
    route_weights,
    expert_gate,
    expert_up,
    expert_down,
):
    seq_count, width = tokens.shape
    positions = key_cache.shape[1]
    heads = gate_cache.shape[1]
    chips = lax.axis_size("ep")
    pieces = chips // EXPERTS
    rows = chips * 2 * CAP
    columns = width // 2
    quarter = columns // 2
    groups = seq_count // GROUP
    swap = [(0, 1), (1, 0)]
    dma = pltpu.SemaphoreType.DMA

    partial_out, slots = pl.pallas_call(
        functools.partial(attention_kernel, pieces),
        name="attention",
        out_shape=(
            jax.ShapeDtypeStruct((seq_count, width), bf16),
            jax.ShapeDtypeStruct((rows, 4 * seq_count), bf16),
        ),
        in_specs=[HBM_SPEC] * 12,
        out_specs=(VMEM_SPEC, VMEM_SPEC),
        scratch_shapes=[
            pltpu.SMEM((seq_count,), jnp.int32),
            pltpu.VMEM((seq_count, width), bf16),
            pltpu.VMEM((1, width), f32),
            pltpu.VMEM((heads, width), bf16),
            pltpu.VMEM((2, seq_count), jnp.int32),
            pltpu.VMEM(query_weight.shape, bf16),
            pltpu.VMEM(key_weight.shape, bf16),
            pltpu.VMEM(value_weight.shape, bf16),
            pltpu.VMEM(out_weight.shape, bf16),
            pltpu.VMEM(key_cache.shape, bf16),
            pltpu.VMEM(value_cache.shape, bf16),
            pltpu.VMEM(gate_cache.shape, f32),
            pltpu.VMEM((seq_count, heads, LANES), f32),
            pltpu.VMEM((seq_count, LANES), f32),
            pltpu.VMEM((seq_count, LANES), f32),
            pltpu.VMEM((heads, LANES), f32),
            pltpu.VMEM((seq_count, heads, LANES), f32),
            dma((5,)),
            dma((4,)),
            dma((groups,)),
            dma((seq_count,)),
            dma((seq_count,)),
        ],
        compiler_params=pltpu.CompilerParams(vmem_limit_bytes=25 << 20),
    )(
        *map(
            in_hbm,
            (
                lengths,
                tokens,
                mix_gain.reshape(1, width),
                forget_weight.T,
                routes.T,
                query_weight,
                key_weight,
                value_weight,
                out_weight,
                key_cache,
                value_cache,
                gate_cache,
            ),
        ),
    )
    other_out = lax.ppermute(partial_out, "tp", swap)

    outgoing, own_half = pl.pallas_call(
        dispatch_kernel,
        name="dispatch",
        out_shape=(
            jax.ShapeDtypeStruct((rows, quarter), bf16),
            jax.ShapeDtypeStruct((seq_count, columns), bf16),
        ),
        in_specs=[VMEM_SPEC] * 5,
        out_specs=(VMEM_SPEC, VMEM_SPEC),
        scratch_shapes=[
            pltpu.VMEM((seq_count, width), bf16),
            pltpu.VMEM((seq_count, width), bf16),
        ],
        compiler_params=pltpu.CompilerParams(vmem_limit_bytes=8 << 20),
    )(tokens, partial_out, other_out, expert_gain.reshape(1, width), slots)

    received = lax.all_to_all(
        outgoing.reshape(chips, 2 * CAP, quarter), "ep", split_axis=0, concat_axis=0, tiled=True
    )
    others = lax.ppermute(received, "tp", swap)

    units = expert_gate.shape[1]
    parts = max(1, units // 512)
    in_rows = chips * CAP
    back_mine, back_others = pl.pallas_call(
        functools.partial(expert_kernel, parts),
        name="experts",
        out_shape=(jax.ShapeDtypeStruct((rows, quarter), bf16),) * 2,
        in_specs=[VMEM_SPEC] * 4 + [HBM_SPEC],
        out_specs=(VMEM_SPEC, VMEM_SPEC),
        scratch_shapes=[
            pltpu.VMEM((in_rows, width), bf16),
            pltpu.VMEM((in_rows, units), bf16),
            pltpu.VMEM((4, units, quarter), bf16),
            dma((4,)),
        ],
        compiler_params=pltpu.CompilerParams(vmem_limit_bytes=20 << 20),
    )(
        received.reshape(rows, quarter),
        others.reshape(rows, quarter),
        in_vmem(expert_gate),
        in_vmem(expert_up),
        in_hbm(expert_down),
    )
    from_other = lax.ppermute(back_others, "tp", swap)
    share = (back_mine.astype(f32) + from_other.astype(f32)).astype(bf16)
    returned = lax.all_to_all(
        share.reshape(chips, 2 * CAP, quarter), "ep", split_axis=0, concat_axis=0, tiled=True
    )
    half = pl.pallas_call(
        combine_kernel,
        name="combine",
        out_shape=jax.ShapeDtypeStruct((seq_count, columns), bf16),
        in_specs=[VMEM_SPEC] * 4,
        out_specs=VMEM_SPEC,
        compiler_params=pltpu.CompilerParams(vmem_limit_bytes=8 << 20),
    )(returned.reshape(rows, quarter), slots, own_half, route_weights.T)
    return lax.all_gather(half, "tp", axis=1, tiled=True)


def solution(mesh):
    return jax.shard_map(
        on_device,
        mesh=mesh,
        in_specs=(
            P("ep", None),
            P("ep"),
            P("ep", None, "tp"),
            P("ep", None, "tp"),
            P("ep", "tp", None),
            P(),
            P(None, "tp"),
            P(None, "tp"),
            P(None, "tp"),
            P(None, "tp"),
            P("tp", None),
            P(),
            P("ep", None),
            P("ep", None),
            P(None, ("ep", "tp")),
            P(None, ("ep", "tp")),
            P(("ep", "tp"), None),
        ),
        out_specs=P("ep", None),
        check_vma=False,
    )
```

time: 169 us -> 64.4 us (0.38)
  waiting for transfers between devices: 40.8 us -> 4.3 us
  matrix products: 34.1 us -> 0 us
  local copies, waits for them, and re-layouts: 33.9 us -> 0.67 us
  Pallas kernels: 0 us -> 19.1 us
  between operations: 13.7 us -> 0.05 us
  blocking collectives: 26.7 us -> 39.2 us
  other arithmetic: 11.7 us -> 0.1 us
  starting transfers between devices: 6.82 us -> 0.77 us
    dot_general x11 -> x0, matrix products: 34.1 us -> none  [the longest x1 10.9 us: expert_work(): jnp.dot(hidden, expert_down, preferred_element_type=jnp.float32)]
    unnamed x23 -> x11, local copies, waits for them, and re-layouts: 25.3 us -> 0.67 us
    psum x1 -> x0, waiting for transfers between devices: 20.2 us -> none  [on_device(): lax.psum(partial_out, 'tp').astype(jnp.float32)]
    pallas_call x0 -> x4, Pallas kernels: none -> 19.1 us  [the longest x1 10.1 us: on_device(): pl.pallas_call(functools.partial(attention_kernel, pieces), name='attenti...]
    all_to_all x1 -> x2, blocking collectives: 22.1 us -> 37.3 us  [the longest x1 20.9 us: on_device(): lax.all_to_all(outgoing.reshape(chips, 2 * CAP, quarter), 'ep', split_axi...]
    all_to_all x1 -> x0, waiting for transfers between devices: 13.8 us -> none  [on_device(): lax.all_to_all(share, 'ep', split_axis=0, concat_axis=0, tiled=True)]
    all_to_all x1 -> x0, starting transfers between devices: 6.78 us -> none  [on_device(): lax.all_to_all(share, 'ep', split_axis=0, concat_axis=0, tiled=True)]
    reduce_scatter x1 -> x0, waiting for transfers between devices: 6.77 us -> none  [on_device(): lax.psum_scatter(partial_rows, 'tp', scatter_dimension=2, tiled=True)]
  transfers between devices with their start and end apart: 3 -> 3, of which waited for: 3 -> 3; matrix products, arithmetic and copies ran while one was open for 1% -> 0% of each run, Pallas kernels for 0% -> 0%
where the time goes in v1:
time: 64.4 us; the launch traced here: 64.2 us
  blocking collectives  39.2 us (61%)
  Pallas kernels  19.1 us (30%)
  waiting for transfers between devices  4.3 us (7%)
  starting transfers between devices  0.77 us (1%)
  local copies, waits for them, and re-layouts  0.67 us (1%)
    all_to_all x1, blocking collectives, on_device(): lax.all_to_all(outgoing.reshape(chips, 2 * CAP, quarter), 'ep', split_axi...  20.9 us
    all_to_all x1, blocking collectives, on_device(): lax.all_to_all(share.reshape(chips, 2 * CAP, quarter), 'ep', split_axis=0...  16.3 us
    pallas_call x1, Pallas kernels, on_device(): pl.pallas_call(functools.partial(attention_kernel, pieces), name='attenti...  10.1 us
    pallas_call x1, Pallas kernels, on_device(): pl.pallas_call(functools.partial(expert_kernel, parts), name='experts', o...  8.33 us
    all_gather x1, blocking collectives, on_device(): return lax.all_gather(half, 'tp', axis=1, tiled=True)  1.9 us
    ppermute x1, waiting for transfers between devices, on_device(): others = lax.ppermute(received, 'tp', swap)  1.72 us
    ppermute x1, waiting for transfers between devices, on_device(): from_other = lax.ppermute(back_others, 'tp', swap)  1.59 us
  transfers between devices with their start and end apart: 3, of which 3 were waited for; matrix products, arithmetic and copies ran while one was open for 0% of the time, Pallas kernels for 0%

profile of v1, /device:TPU:0, one launch (start us, length us, event | category | flops | bytes accessed | tf_op | source)
XLA Modules:
  0.0 64.2 jit_solution(884369010799641755)
XLA Ops:
  0.0 0.0 copy-start.2
  0.0 0.0 copy-start.3
  0.0 0.0 copy-start
  0.0 0.0 copy-start.1
  0.0 10.1 %attention.1 = (bf16[32,2048]{1,0:T(8,128)(2,1)S(1)}, bf16[384,128]{1,0:T(8,128)(2,1)S(1)}) custom-call(s32[32]{0:T(128)} %lengths_in.1, bf16[32,2048]{1,0:T(8,128)(2,1)} %tokens.3, f32[1,2048]{1,0:T(1,128)} %bitcast.18, bf16[8,2048]{1,0:T(8,128)(2,1)} %bitcast.17, s32[2,32]{1,0:T(2,128)} %bitcast.19, bf16[2048,512]{1,0:T(8,128)(2,1)} %wq.1, ...), custom_call_target="tpu_custom_call" | custom-call | tf_op jit(solution)/shard_map/attention/pallas_call | solution.py:399
  10.1 0.6 collective-permute-start
  10.7 1.0 %collective-permute-done.other = bf16[32,2048]{1,0:T(8,128)(2,1)S(1)} collective-permute-done((bf16[32,2048]{1,0:T(8,128)(2,1)S(1)}, bf16[32,2048]{1,0:T(8,128)(2,1)S(1)}, u32[]{:S(2)}, u32[]{:S(2)}) %collective-permute-start) | collective-permute-done | bytes 131104 | tf_op jit(solution)/shard_map/ppermute | solution.py:452
  11.7 0.0 copy-done.2
  11.7 0.0 copy-done.3
  11.7 0.4 dispatch.1
  12.1 20.9 %all_to_all.10 = bf16[16,24,512]{2,1,0:T(8,128)(2,1)S(1)} all-to-all(bf16[16,24,512]{2,1,0:T(8,128)(2,1)S(1)} %bitcast.12), channel_id=1, replica_groups=mesh['ep'=16,'tp'=2] {'ep'}, dimensions={0} | all-to-all | bytes 786432 | tf_op jit(solution)/shard_map/all_to_all | solution.py:470
  33.1 0.0 collective-permute-start.1
  33.1 1.7 %collective-permute-done.1 = bf16[16,24,512]{2,1,0:T(8,128)(2,1)S(1)} collective-permute-done((bf16[16,24,512]{2,1,0:T(8,128)(2,1)S(1)}, bf16[16,24,512]{2,1,0:T(8,128)(2,1)S(1)}, u32[]{:S(2)}, u32[]{:S(2)}) %collective-permute-start.1) | collective-permute-done | bytes 393248 | tf_op jit(solution)/shard_map/ppermute | solution.py:473
  34.8 0.0 copy-done
  34.8 0.0 copy-done.1
  34.8 0.0 copy-start.4
  34.8 8.3 %experts.1 = (bf16[384,512]{1,0:T(8,128)(2,1)S(1)}, bf16[384,512]{1,0:T(8,128)(2,1)S(1)}) custom-call(bf16[384,512]{1,0:T(8,128)(2,1)S(1)} %bitcast.11, bf16[384,512]{1,0:T(8,128)(2,1)S(1)} %bitcast.13, bf16[2048,2048]{1,0:T(8,128)(2,1)S(1)} %copy-done, bf16[2048,2048]{1,0:T(8,128)(2,1)S(1)} %copy-done.1, bf16[2048,2048]{1,0:T(8,128)(2,1)} %w_down.1), custom_call_target="tpu_custom_call" | custom-call | tf_op jit(solution)/shard_map/experts/pallas_call | solution.py:478
  43.1 0.2 collective-permute-start.2
  43.3 1.6 %collective-permute-done.2 = bf16[384,512]{1,0:T(8,128)(2,1)S(1)} collective-permute-done((bf16[384,512]{1,0:T(8,128)(2,1)S(1)}, bf16[384,512]{1,0:T(8,128)(2,1)S(1)}, u32[]{:S(2)}, u32[]{:S(2)}) %collective-permute-start.2) | collective-permute-done | bytes 393248 | tf_op jit(solution)/shard_map/ppermute | solution.py:498
  44.9 0.1 add_convert_fusion
  45.0 16.3 %all_to_all.11 = bf16[16,24,512]{2,1,0:T(8,128)(2,1)S(1)} all-to-all(bf16[16,24,512]{2,1,0:T(8,128)(2,1)S(1)} %bitcast.16), channel_id=1, replica_groups=mesh['ep'=16,'tp'=2] {'ep'}, dimensions={0} | all-to-all | bytes 786432 | tf_op jit(solution)/shard_map/all_to_all | solution.py:500
  61.3 0.0 copy-done.4
  61.4 0.3 combine.1
  61.6 1.9 %all_gather.3 = bf16[32,2048]{1,0:T(8,128)(2,1)S(1)} all-gather(bf16[32,1024]{1,0:T(8,128)(2,1)S(1)} %combine.1), channel_id=1, replica_groups=mesh['ep'=16,'tp'=2] {'tp'}, dimensions={1}, use_global_device_ids=true | all-gather | bytes 196608 | tf_op jit(solution)/shard_map/all_gather | solution.py:511
  63.5 0.7 %copy.19 = bf16[32,2048]{1,0:T(8,128)(2,1)} copy(bf16[32,2048]{1,0:T(8,128)(2,1)S(1)} %all_gather.3) | data formatting | bytes 262144
Async XLA Ops:
  0.0 11.7 %copy-start.2 = (bf16[32,2048]{1,0:T(8,128)(2,1)S(1)}, bf16[32,2048]{1,0:T(8,128)(2,1)}, u32[]{:S(2)}) copy-start(bf16[32,2048]{1,0:T(8,128)(2,1)} %tokens.3) | copy-start | bytes 393220
  0.0 11.7 %copy-start.3 = (f32[2048]{0:T(1024)S(1)}, f32[2048]{0:T(1024)}, u32[]{:S(2)}) copy-start(f32[2048]{0:T(1024)} %param.28) | copy-start | bytes 24580
  0.0 34.8 %copy-start = (bf16[2048,2048]{1,0:T(8,128)(2,1)S(1)}, bf16[2048,2048]{1,0:T(8,128)(2,1)}, u32[]{:S(2)}) copy-start(bf16[2048,2048]{1,0:T(8,128)(2,1)} %w_gate.1) | copy-start | bytes 25165828
  0.0 34.8 %copy-start.1 = (bf16[2048,2048]{1,0:T(8,128)(2,1)S(1)}, bf16[2048,2048]{1,0:T(8,128)(2,1)}, u32[]{:S(2)}) copy-start(bf16[2048,2048]{1,0:T(8,128)(2,1)} %w_up.1) | copy-start | bytes 25165828
  10.1 1.6 %collective-permute-start = (bf16[32,2048]{1,0:T(8,128)(2,1)S(1)}, bf16[32,2048]{1,0:T(8,128)(2,1)S(1)}, u32[]{:S(2)}, u32[]{:S(2)}) collective-permute-start(bf16[32,2048]{1,0:T(8,128)(2,1)S(1)} %get-tuple-element.11.own), channel_id=1, source_target_pairs={{0,1},{1,0},{2,3},{3,2},{4,5},{5,4},{6,7},{7,6},{8,9},{9,8},{10,11... | collective-permute-start | bytes 393224 | tf_op jit(solution)/shard_map/ppermute | solution.py:452
  33.1 1.7 %collective-permute-start.1 = (bf16[16,24,512]{2,1,0:T(8,128)(2,1)S(1)}, bf16[16,24,512]{2,1,0:T(8,128)(2,1)S(1)}, u32[]{:S(2)}, u32[]{:S(2)}) collective-permute-start(bf16[16,24,512]{2,1,0:T(8,128)(2,1)S(1)} %all_to_all.10), channel_id=1, source_target_pairs={{0,1},{1,0},{2,3},{3,2},{4,5},{5,4},{6,7},{7,6},{8,9},{9,8},{10,11... | collective-permute-start | bytes 1179656 | tf_op jit(solution)/shard_map/ppermute | solution.py:473
  34.8 26.6 %copy-start.4 = (f32[32,2]{0,1:T(2,128)S(1)}, f32[32,2]{0,1:T(2,128)}, u32[]{:S(2)}) copy-start(f32[32,2]{0,1:T(2,128)} %param.30) | copy-start | bytes 772
  43.1 1.8 %collective-permute-start.2 = (bf16[384,512]{1,0:T(8,128)(2,1)S(1)}, bf16[384,512]{1,0:T(8,128)(2,1)S(1)}, u32[]{:S(2)}, u32[]{:S(2)}) collective-permute-start(bf16[384,512]{1,0:T(8,128)(2,1)S(1)} %get-tuple-element.15), channel_id=1, source_target_pairs={{0,1},{1,0},{2,3},{3,2},{4,5},{5,4},{6,7},{7,6},{8,9},{9,8},{10,11... | collective-permute-start | bytes 1179656 | tf_op jit(solution)/shard_map/ppermute | solution.py:498

commit v2 on v1

--- a/solution.py
+++ b/solution.py
@@ -13,6 +13,7 @@
 LANES = 128
 GROUP = 8
 STEP = 128
+COVER = 10**12
 
 eps = 1e-06
 f32 = jnp.float32
@@ -65,11 +66,25 @@
     return hit.astype(bf16)
 
 
+def sort_table(row):
+    count = row.shape[1]
+    lane, sub = iota((count, count), 1), iota((count, count), 0)
+    column = jnp.sum(jnp.where(lane == sub, row, 0), axis=1, keepdims=True)
+    before = (row > column) | ((row == column) & (lane < sub))
+    rank = jnp.sum(before.astype(f32), axis=1, keepdims=True)
+    lane, sub = iota((count, LANES), 1), iota((count, LANES), 0)
+    hit = rank == lane.astype(f32)
+    order = jnp.sum(jnp.where(hit, sub, 0), axis=0, keepdims=True)
+    length = jnp.sum(jnp.where(hit, column, 0), axis=0, keepdims=True)
+    return order, length
+
+
 def attention_kernel(
     pieces,
-    lengths_in,
+    lengths,
     tokens,
     gain,
+    second_gain,
     forget,
     routes,
     wq,
@@ -81,8 +96,11 @@
     gates,
     partial_out,
     slots,
-    lengths_s,
     tokens_v,
+    second_gain_v,
+    lengths_v,
+    table_v,
+    table_s,
     gain_v,
     forget_v,
     routes_v,
@@ -100,7 +118,7 @@
     mixed_v,
     small_sem,
     weight_sem,
-    gate_sem,
+    base_sem,
     key_sem,
     value_sem,
 ):
@@ -109,76 +127,79 @@
     pairs = heads // 2
     groups = seq_count // GROUP
 
-    lengths = lengths_s
     small = [
         pltpu.make_async_copy(src, dst, small_sem.at[i])
         for i, (src, dst) in enumerate(
             (
-                (lengths_in, lengths_s),
-                (routes, routes_v),
+                (lengths, lengths_v),
                 (tokens, tokens_v),
                 (gain, gain_v),
                 (forget, forget_v),
+                (routes, routes_v),
+                (second_gain, second_gain_v),
             )
         )
     ]
+    table_copy = pltpu.make_async_copy(table_v, table_s, small_sem.at[6])
     copies = [
         pltpu.make_async_copy(src, dst, weight_sem.at[i])
         for i, (src, dst) in enumerate(((wq, wq_v), (wk, wk_v), (wv, wv_v), (wo, wo_v)))
     ]
 
-    def used(s):
-        return pl.multiple_of((lengths[s] + STEP - 1) // STEP * STEP, STEP)
-
-    def key_copy(s):
-        window = pl.ds(0, used(s))
-        return pltpu.make_async_copy(keys.at[s, window], keys_v.at[s, window], key_sem.at[s])
-
-    def value_copy(s):
-        window = pl.ds(0, used(s))
-        return pltpu.make_async_copy(values.at[s, window], values_v.at[s, window], value_sem.at[s])
-
-    def gate_copy(g):
-        window = pl.ds(g * GROUP, GROUP)
-        return pltpu.make_async_copy(gates.at[window], gates_v.at[window], gate_sem.at[g])
-
-    for c in small + copies[:3]:
+    every = pl.ds(0, seq_count)
+    base = pl.ds(0, STEP)
+    gate_copy = pltpu.make_async_copy(gates, gates_v, base_sem.at[0])
+    key_base = pltpu.make_async_copy(keys.at[every, base], keys_v.at[every, base], base_sem.at[1])
+    value_base = pltpu.make_async_copy(
+        values.at[every, base], values_v.at[every, base], base_sem.at[2]
+    )
+
+    def chunks(g):
+        return (table_s[1, g * GROUP] + STEP - 1) // STEP
+
+    def group_copies(g):
+        window = pl.ds(STEP, pl.multiple_of((chunks(g) - 1) * STEP, STEP))
+        pairs_of = []
+        for j in range(GROUP):
+            s = table_s[0, g * GROUP + j]
+            pairs_of.append(
+                (
+                    pltpu.make_async_copy(keys.at[s, window], keys_v.at[s, window], key_sem.at[s]),
+                    pltpu.make_async_copy(
+                        values.at[s, window], values_v.at[s, window], value_sem.at[s]
+                    ),
+                )
+            )
+        return pairs_of
+
+    for c in small + copies[:3] + [gate_copy, key_base, value_base, copies[3]]:
         c.start()
-
-    def start_keys(g):
-        gate_copy(g).start()
-        for j in range(GROUP):
-            key_copy(g * GROUP + j).start()
-
-    def start_values(g):
-        for j in range(GROUP):
-            value_copy(g * GROUP + j).start()
-
     small[0].wait()
-    start_keys(0)
-
-    def clear(s, _):
-        values_v[s] = jnp.zeros(values_v.shape[1:], bf16)
+    order, length = sort_table(lengths_v[...])
+    table_v[0:1, :] = order
+    table_v[1:2, :] = length
+    table_copy.start()
+    table_copy.wait()
+
+    def start_group(g, _):
+        @pl.when(chunks(g) > 1)
+        def _():
+            copies_of = group_copies(g)
+            for key_copy, _ in copies_of:
+                key_copy.start()
+            for _, value_copy in copies_of:
+                value_copy.start()
+
         return 0
 
-    lax.fori_loop(0, seq_count, clear, 0)
-    start_values(0)
-
-    def start_rest(g, _):
-        start_keys(g)
-        start_values(g)
-        return 0
-
-    lax.fori_loop(1, groups, start_rest, 0)
-    copies[3].start()
+    lax.fori_loop(0, groups, start_group, 0)
 
     for c in small[1:]:
         c.wait()
-    slots[...] = slot_matrix(routes_v[...], slots.shape[0], pieces)
-
     normal_in = normed(tokens_v[...], gain_v[...]).astype(bf16)
     gate_in = lax.dot_general(forget_v[...], normal_in, NT, preferred_element_type=f32)
     log_gate_v[:, :seq_count] = jnp.minimum(gate_in, 0.0) - jnp.log1p(jnp.exp(-jnp.abs(gate_in)))
+    slots[...] = slot_matrix(routes_v[...], slots.shape[0], pieces)
     low = iota((seq_count, LANES), 1) < HD
     for c in copies[:3]:
         c.wait()
@@ -201,20 +222,16 @@
         query_v[:, 2 * j + 1, :] = two
 
     lane = iota((heads, LANES), 1)
-    position = iota((heads, positions), 1)
-
-    def group_step(g, _):
-        gate_copy(g).wait()
+
+    def attend(g, reach):
+        position = iota((heads, reach), 1)
         scored = []
         for j in range(GROUP):
-            s = g * GROUP + j
-            key_copy(s).wait()
-        for j in range(GROUP):
-            s = g * GROUP + j
-            length = lengths[s]
+            i = g * GROUP + j
+            s, length = table_s[0, i], table_s[1, i]
             query_s = query_v[s]
             score = lax.dot_general(
-                query_s.astype(bf16), keys_v[s], NT, preferred_element_type=f32
+                query_s.astype(bf16), keys_v[s, :reach], NT, preferred_element_type=f32
             )
             last = length - 1
             start = pl.multiple_of(last // LANES * LANES, LANES)
@@ -224,21 +241,32 @@
             )
             offset = jnp.sum(picked, axis=1, keepdims=True)
             own = jnp.sum(query_s * key_new_v[pl.ds(s, 1), :], axis=1, keepdims=True)
-            score = jnp.where(position < length, score + offset - gates_v[s], -jnp.inf)
+            score = jnp.where(position < length, score + offset - gates_v[s, :, :reach], -jnp.inf)
             highest = jnp.maximum(jnp.max(score, axis=1, keepdims=True), own)
             raised = jnp.exp(score - highest)
             own_raised = jnp.exp(own - highest)
             total = jnp.sum(raised, axis=1, keepdims=True) + own_raised
-            scored.append((raised.astype(bf16), own_raised, total))
+            scored.append((s, raised.astype(bf16), own_raised, total))
         for j in range(GROUP):
-            s = g * GROUP + j
-            value_copy(s).wait()
-        for j in range(GROUP):
-            s = g * GROUP + j
-            raised, own_raised, total = scored[j]
-            product = jnp.dot(raised, values_v[s], preferred_element_type=f32)
+            s, raised, own_raised, total = scored[j]
+            product = jnp.dot(raised, values_v[s, :reach], preferred_element_type=f32)
             product = product + own_raised * value_new_v[pl.ds(s, 1), :]
             mixed_v[s] = product / total
+
+    for c in (gate_copy, key_base, value_base):
+        c.wait()
+
+    def group_step(g, _):
+        count = chunks(g)
+
+        @pl.when(count > 1)
+        def _():
+            for key_copy, value_copy in group_copies(g):
+                key_copy.wait()
+                value_copy.wait()
+
+        for n in range(1, positions // STEP + 1):
+            pl.when(count == n)(functools.partial(attend, g, n * STEP))
         return 0
 
     lax.fori_loop(0, groups, group_step, 0)
@@ -279,73 +307,78 @@
     return (target == iota(shape, 1 - dim).astype(f32)).astype(f32).astype(bf16)
 
 
-def expert_kernel(
-    parts,
-    mine,
-    others,
-    w_gate,
-    w_up,
-    w_down,
-    out_mine,
-    out_others,
-    rows_v,
-    hidden_v,
-    down_v,
-    down_sem,
-):
-    width, units = w_gate.shape
+def unpack_rows(source, rows_v):
+    quarter = source.shape[1]
+    rows_in = source.shape[0]
+    span = min(rows_in, 16 * 2 * CAP)
+    for half in range(2):
+        matrix = gather_matrix(span, span // 2, half, False)
+        for piece in range(rows_in // span):
+            rows_v[
+                piece * (span // 2) : (piece + 1) * (span // 2),
+                half * quarter : (half + 1) * quarter,
+            ] = jnp.dot(
+                matrix, source[piece * span : (piece + 1) * span, :], preferred_element_type=f32
+            ).astype(bf16)
+
+
+def down_rows(hidden, w_down, target, side, quarter):
+    rows_in = target.shape[0]
+    span = min(rows_in, 16 * 2 * CAP)
+    results = []
+    for half in range(2):
+        start = pl.multiple_of(side * 2 * quarter + half * quarter, quarter)
+        results.append(
+            jnp.dot(
+                hidden[...], w_down[:, pl.ds(start, quarter)], preferred_element_type=f32
+            ).astype(bf16)
+        )
+    spread = [gather_matrix(span, span // 2, half, True) for half in range(2)]
+    for piece in range(rows_in // span):
+        taken = slice(piece * (span // 2), (piece + 1) * (span // 2))
+        target[piece * span : (piece + 1) * span, :] = (
+            jnp.dot(spread[0], results[0][taken], preferred_element_type=f32)
+            + jnp.dot(spread[1], results[1][taken], preferred_element_type=f32)
+        ).astype(bf16)
+
+
+def first_kernel(parts, mine, w_gate, w_up, partial, rows_v):
+    units = w_gate.shape[1]
+    columns = rows_v.shape[1]
     block = units // parts
-    columns = width // 2
-    quarter = columns // 2
-    me = lax.axis_index("tp")
-
-    def down_start(q):
-        return pl.multiple_of(jnp.where(q < 2, 1 - me, me) * columns + (q % 2) * quarter, quarter)
-
-    def down_copy(q):
-        window = pl.ds(down_start(q), quarter)
-        return pltpu.make_async_copy(w_down.at[:, window], down_v.at[q], down_sem.at[q])
-
-    for q in range(4):
-        down_copy(q).start()
-
-    rows_in = mine.shape[0]
-    rows_out = rows_in // 2
-    span = min(rows_in, 16 * 2 * CAP)
-    span_out = span // 2
-    for half in range(2):
-        matrix = gather_matrix(span, span_out, half, False)
-        for piece in range(rows_in // span):
-            taken = pl.ds(piece * span, span)
-            given = pl.ds(piece * span_out, span_out)
-            for source, side in ((mine, me), (others, 1 - me)):
-                start = pl.multiple_of(side * columns + half * quarter, quarter)
-                rows_v[given, pl.ds(start, quarter)] = jnp.dot(
-                    matrix, source[taken, :], preferred_element_type=f32
-                ).astype(bf16)
-
+    rows = pl.ds(pl.multiple_of(lax.axis_index("tp") * columns, columns), columns)
+    unpack_rows(mine, rows_v)
     for j in range(parts):
         window = slice(j * block, (j + 1) * block)
-        gate_out = jnp.dot(rows_v[...], w_gate[:, window], preferred_element_type=f32)
-        up_out = jnp.dot(rows_v[...], w_up[:, window], preferred_element_type=f32)
+        for k, weight in enumerate((w_gate, w_up)):
+            partial[k, :, window] = jnp.dot(
+                rows_v[...], weight[rows, window], preferred_element_type=f32
+            )
+
+
+def second_kernel(
+    parts, others, partial, w_gate, w_up, w_down, hidden_out, out_others, rows_v
+):
+    units = w_gate.shape[1]
+    columns = rows_v.shape[1]
+    block = units // parts
+    side = 1 - lax.axis_index("tp")
+    rows = pl.ds(pl.multiple_of(side * columns, columns), columns)
+    unpack_rows(others, rows_v)
+    for j in range(parts):
+        window = slice(j * block, (j + 1) * block)
+        gate_out, up_out = [
+            partial[k, :, window]
+            + jnp.dot(rows_v[...], weight[rows, window], preferred_element_type=f32)
+            for k, weight in enumerate((w_gate, w_up))
+        ]
         hidden = gate_out * jax.nn.sigmoid(gate_out) * up_out
-        hidden_v[:, j * block : (j + 1) * block] = hidden.astype(bf16)
-
-    spread = [gather_matrix(span, span_out, half, True) for half in range(2)]
-    for side, target in ((0, out_others), (1, out_mine)):
-        results = []
-        for half in range(2):
-            q = 2 * side + half
-            down_copy(q).wait()
-            results.append(
-                jnp.dot(hidden_v[...], down_v[q], preferred_element_type=f32).astype(bf16)
-            )
-        for piece in range(rows_in // span):
-            taken = slice(piece * span_out, (piece + 1) * span_out)
-            target[pl.ds(piece * span, span), :] = (
-                jnp.dot(spread[0], results[0][taken], preferred_element_type=f32)
-                + jnp.dot(spread[1], results[1][taken], preferred_element_type=f32)
-            ).astype(bf16)
+        hidden_out[:, window] = hidden.astype(bf16)
+    down_rows(hidden_out, w_down, out_others, side, others.shape[1])
+
+
+def third_kernel(hidden, w_down, out_mine):
+    down_rows(hidden, w_down, out_mine, lax.axis_index("tp"), out_mine.shape[1])
 
 
 def combine_kernel(returned, slots, own_half, route_weights, out):
@@ -363,6 +396,23 @@
         mixture = mixture + picked[base + seq_count : base + 2 * seq_count] * weights[1]
         span = slice(half * quarter, (half + 1) * quarter)
         out[:, span] = (own_half[:, span].astype(f32) + mixture).astype(bf16)
+
+
+def join_kernel(half, other, out, sem):
+    columns = half.shape[1]
+    me = lax.axis_index("tp")
+    copies = [
+        pltpu.make_async_copy(
+            source,
+            out.at[:, pl.ds(pl.multiple_of(side * columns, columns), columns)],
+            sem.at[i],
+        )
+        for i, (source, side) in enumerate(((half, me), (other, 1 - me)))
+    ]
+    for c in copies:
+        c.start()
+    for c in copies:
+        c.wait()
 
 
 def on_device(
@@ -392,22 +442,24 @@
     rows = chips * 2 * CAP
     columns = width // 2
     quarter = columns // 2
-    groups = seq_count // GROUP
     swap = [(0, 1), (1, 0)]
     dma = pltpu.SemaphoreType.DMA
 
-    partial_out, slots = pl.pallas_call(
+    partial_out, slots, tokens_out, gain_out = pl.pallas_call(
         functools.partial(attention_kernel, pieces),
         name="attention",
         out_shape=(
-            jax.ShapeDtypeStruct((seq_count, width), bf16),
-            jax.ShapeDtypeStruct((rows, 4 * seq_count), bf16),
+            pltpu.VMEM((seq_count, width), bf16),
+            pltpu.VMEM((rows, 4 * seq_count), bf16),
+            pltpu.VMEM((seq_count, width), bf16),
+            pltpu.VMEM((1, width), f32),
         ),
-        in_specs=[HBM_SPEC] * 12,
-        out_specs=(VMEM_SPEC, VMEM_SPEC),
+        in_specs=[HBM_SPEC] * 13,
+        out_specs=(VMEM_SPEC,) * 4,
         scratch_shapes=[
-            pltpu.SMEM((seq_count,), jnp.int32),
-            pltpu.VMEM((seq_count, width), bf16),
+            pltpu.VMEM((1, seq_count), jnp.int32),
+            pltpu.VMEM((2, LANES), jnp.int32),
+            pltpu.SMEM((2, LANES), jnp.int32),
             pltpu.VMEM((1, width), f32),
             pltpu.VMEM((heads, width), bf16),
             pltpu.VMEM((2, seq_count), jnp.int32),
@@ -423,20 +475,21 @@
             pltpu.VMEM((seq_count, LANES), f32),
             pltpu.VMEM((heads, LANES), f32),
             pltpu.VMEM((seq_count, heads, LANES), f32),
-            dma((5,)),
+            dma((7,)),
             dma((4,)),
-            dma((groups,)),
+            dma((3,)),
             dma((seq_count,)),
             dma((seq_count,)),
         ],
-        compiler_params=pltpu.CompilerParams(vmem_limit_bytes=25 << 20),
+        compiler_params=pltpu.CompilerParams(vmem_limit_bytes=59 << 20),
     )(
         *map(
             in_hbm,
             (
-                lengths,
+                lengths.reshape(1, seq_count),
                 tokens,
                 mix_gain.reshape(1, width),
+                expert_gain.reshape(1, width),
                 forget_weight.T,
                 routes.T,
                 query_weight,
@@ -454,6 +507,9 @@
     outgoing, own_half = pl.pallas_call(
         dispatch_kernel,
         name="dispatch",
+        cost_estimate=pl.CostEstimate(
+            flops=COVER, transcendentals=seq_count, bytes_accessed=8 * tokens.size
+        ),
         out_shape=(
             jax.ShapeDtypeStruct((rows, quarter), bf16),
             jax.ShapeDtypeStruct((seq_count, columns), bf16),
@@ -464,8 +520,8 @@
             pltpu.VMEM((seq_count, width), bf16),
             pltpu.VMEM((seq_count, width), bf16),
         ],
-        compiler_params=pltpu.CompilerParams(vmem_limit_bytes=8 << 20),
-    )(tokens, partial_out, other_out, expert_gain.reshape(1, width), slots)
+        compiler_params=pltpu.CompilerParams(vmem_limit_bytes=6 << 20),
+    )(tokens_out, partial_out, other_out, gain_out, slots)
 
     received = lax.all_to_all(
         outgoing.reshape(chips, 2 * CAP, quarter), "ep", split_axis=0, concat_axis=0, tiled=True
@@ -475,26 +531,40 @@
     units = expert_gate.shape[1]
     parts = max(1, units // 512)
     in_rows = chips * CAP
-    back_mine, back_others = pl.pallas_call(
-        functools.partial(expert_kernel, parts),
-        name="experts",
-        out_shape=(jax.ShapeDtypeStruct((rows, quarter), bf16),) * 2,
-        in_specs=[VMEM_SPEC] * 4 + [HBM_SPEC],
+    gate_v, up_v, down_v = in_vmem(expert_gate), in_vmem(expert_up), in_vmem(expert_down)
+    expert_params = pltpu.CompilerParams(vmem_limit_bytes=(3 << 20) + 8 * in_rows * width)
+    partial = pl.pallas_call(
+        functools.partial(first_kernel, parts),
+        name="first",
+        cost_estimate=pl.CostEstimate(
+            flops=2 * in_rows * width * units, transcendentals=0, bytes_accessed=2 * expert_up.size
+        ),
+        out_shape=pltpu.VMEM((2, in_rows, units), f32),
+        in_specs=[VMEM_SPEC] * 3,
+        out_specs=VMEM_SPEC,
+        scratch_shapes=[pltpu.VMEM((in_rows, columns), bf16)],
+        compiler_params=expert_params,
+    )(received.reshape(rows, quarter), gate_v, up_v)
+    hidden, back_others = pl.pallas_call(
+        functools.partial(second_kernel, parts),
+        name="second",
+        out_shape=(pltpu.VMEM((in_rows, units), bf16), pltpu.VMEM((rows, quarter), bf16)),
+        in_specs=[VMEM_SPEC] * 5,
         out_specs=(VMEM_SPEC, VMEM_SPEC),
-        scratch_shapes=[
-            pltpu.VMEM((in_rows, width), bf16),
-            pltpu.VMEM((in_rows, units), bf16),
-            pltpu.VMEM((4, units, quarter), bf16),
-            dma((4,)),
-        ],
-        compiler_params=pltpu.CompilerParams(vmem_limit_bytes=20 << 20),
-    )(
-        received.reshape(rows, quarter),
-        others.reshape(rows, quarter),
-        in_vmem(expert_gate),
-        in_vmem(expert_up),
-        in_hbm(expert_down),
-    )
+        scratch_shapes=[pltpu.VMEM((in_rows, columns), bf16)],
+        compiler_params=expert_params,
+    )(others.reshape(rows, quarter), partial, gate_v, up_v, down_v)
+    back_mine = pl.pallas_call(
+        third_kernel,
+        name="third",
+        cost_estimate=pl.CostEstimate(
+            flops=in_rows * width * units, transcendentals=0, bytes_accessed=expert_up.size
+        ),
+        out_shape=pltpu.VMEM((rows, quarter), bf16),
+        in_specs=[VMEM_SPEC] * 2,
+        out_specs=VMEM_SPEC,
+        compiler_params=expert_params,
+    )(hidden, down_v)
     from_other = lax.ppermute(back_others, "tp", swap)
     share = (back_mine.astype(f32) + from_other.astype(f32)).astype(bf16)
     returned = lax.all_to_all(
@@ -503,12 +573,21 @@
     half = pl.pallas_call(
         combine_kernel,
         name="combine",
-        out_shape=jax.ShapeDtypeStruct((seq_count, columns), bf16),
+        out_shape=pltpu.VMEM((seq_count, columns), bf16),
         in_specs=[VMEM_SPEC] * 4,
         out_specs=VMEM_SPEC,
-        compiler_params=pltpu.CompilerParams(vmem_limit_bytes=8 << 20),
+        compiler_params=pltpu.CompilerParams(vmem_limit_bytes=6 << 20),
     )(returned.reshape(rows, quarter), slots, own_half, route_weights.T)
-    return lax.all_gather(half, "tp", axis=1, tiled=True)
+    other_half = lax.ppermute(half, "tp", swap)
+    return pl.pallas_call(
+        join_kernel,
+        name="join",
+        out_shape=jax.ShapeDtypeStruct((seq_count, width), bf16),
+        in_specs=[VMEM_SPEC] * 2,
+        out_specs=HBM_SPEC,
+        scratch_shapes=[dma((2,))],
+        compiler_params=pltpu.CompilerParams(vmem_limit_bytes=1 << 20),
+    )(half, other_half)
 
 
 def solution(mesh):

time: 64.4 us -> 58.9 us (0.915)
  Pallas kernels: 19.1 us -> 16.9 us
  waiting for transfers between devices: 4.3 us -> 2.23 us
  blocking collectives: 39.2 us -> 38 us
    all_gather x1 -> x0, blocking collectives: 1.9 us -> none  [on_device(): return lax.all_gather(half, 'tp', axis=1, tiled=True)]
    ppermute x1, waiting for transfers between devices: 1.72 us -> 0.01 us  [on_device(): others = lax.ppermute(received, 'tp', swap)]
    ppermute x1, waiting for transfers between devices: 1.59 us -> 0.01 us  [on_device(): from_other = lax.ppermute(back_others, 'tp', swap)]
    ppermute x0 -> x1, waiting for transfers between devices: none -> 1.24 us  [on_device(): other_half = lax.ppermute(half, 'tp', swap)]
    pallas_call x3 -> x6, Pallas kernels: 9.01 us -> 7.86 us  [the longest x1 3.18 us: on_device(): pl.pallas_call(functools.partial(second_kernel, parts), name='second', ou...]
    pallas_call x1, Pallas kernels: 10.1 us -> 9.09 us  [on_device(): pl.pallas_call(functools.partial(attention_kernel, pieces), name='attenti...]
  transfers between devices with their start and end apart: 3 -> 4, of which waited for: 3 -> 2; matrix products, arithmetic and copies ran while one was open for 0% -> 0% of each run, Pallas kernels for 0% -> 6%
where the time goes in v2:
time: 58.9 us; the launch traced here: 58.8 us
  blocking collectives  38 us (65%)
  Pallas kernels  16.9 us (29%)
  waiting for transfers between devices  2.23 us (4%)
  starting transfers between devices  1.2 us (2%)
    all_to_all x1, blocking collectives, on_device(): lax.all_to_all(outgoing.reshape(chips, 2 * CAP, quarter), 'ep', split_axi...  21.5 us
    all_to_all x1, blocking collectives, on_device(): lax.all_to_all(share.reshape(chips, 2 * CAP, quarter), 'ep', split_axis=0...  16.5 us
    pallas_call x1, Pallas kernels, on_device(): pl.pallas_call(functools.partial(attention_kernel, pieces), name='attenti...  9.09 us
    pallas_call x1, Pallas kernels, on_device(): pl.pallas_call(functools.partial(second_kernel, parts), name='second', ou...  3.18 us
    pallas_call x1, Pallas kernels, on_device(): pl.pallas_call(functools.partial(first_kernel, parts), name='first', cost...  1.99 us
    pallas_call x1, Pallas kernels, on_device(): pl.pallas_call(third_kernel, name='third', cost_estimate=pl.CostEstimate(...  1.35 us
    ppermute x1, waiting for transfers between devices, on_device(): other_half = lax.ppermute(half, 'tp', swap)  1.24 us
  transfers between devices with their start and end apart: 4, of which 2 were waited for; matrix products, arithmetic and copies ran while one was open for 0% of the time, Pallas kernels for 6%

profile of v2, /device:TPU:0, one launch (start us, length us, event | category | flops | bytes accessed | tf_op | source)
XLA Modules:
  0.0 58.8 jit_solution(17774538928568369946)
XLA Ops:
  0.0 9.1 %attention.1 = (bf16[32,2048]{1,0:T(8,128)(2,1)S(1)}, bf16[384,128]{1,0:T(8,128)(2,1)S(1)}, bf16[32,2048]{1,0:T(8,128)(2,1)S(1)}, f32[1,2048]{1,0:T(1,128)S(1)}) custom-call(s32[1,32]{1,0:T(1,128)} %bitcast.23, bf16[32,2048]{1,0:T(8,128)(2,1)} %tokens.1, f32[1,2048]{1,0:T(1,128)} %bitcast.20, f32[1,2048]{1,0:T(1,128)} %bitcast.21, bf16[8,2048]{1,0:T(8,128)(2,1)} %bitcast.19, ...), custom_call_target="tpu_custom_call" | custom-call | tf_op jit(solution)/shard_map/attention/pallas_call | solution.py:448
  9.1 0.6 collective-permute-start
  9.7 1.0 %collective-permute-done.other = bf16[32,2048]{1,0:T(8,128)(2,1)S(1)} collective-permute-done((bf16[32,2048]{1,0:T(8,128)(2,1)S(1)}, bf16[32,2048]{1,0:T(8,128)(2,1)S(1)}, u32[]{:S(2)}, u32[]{:S(2)}) %collective-permute-start) | collective-permute-done | bytes 131104 | tf_op jit(solution)/shard_map/ppermute | solution.py:505
  10.6 0.0 copy-start
  10.6 0.0 copy-start.1
  10.6 0.4 dispatch.1
  11.1 0.0 slice-start
  11.1 21.5 %all_to_all.10 = bf16[16,24,512]{2,1,0:T(8,128)(2,1)S(1)} all-to-all(bf16[16,24,512]{2,1,0:T(8,128)(2,1)S(1)} %bitcast.16), channel_id=1, replica_groups=mesh['ep'=16,'tp'=2] {'ep'}, dimensions={0} | all-to-all | bytes 786432 | tf_op jit(solution)/shard_map/all_to_all | solution.py:526
  32.6 0.0 collective-permute-start.1
  32.6 0.0 copy-done
  32.6 0.0 copy-done.1
  32.6 0.0 slice-start.1
  32.6 2.0 %first.1.partial = f32[2,192,2048]{2,1,0:T(8,128)S(1)} custom-call(bf16[384,512]{1,0:T(8,128)(2,1)S(1)} %bitcast.14, bf16[2048,2048]{1,0:T(8,128)(2,1)S(1)} %copy-done, bf16[2048,2048]{1,0:T(8,128)(2,1)S(1)} %copy-done.1), custom_call_target="tpu_custom_call" | custom-call | flops 1610612736 | bytes 8388608 | tf_op jit(solution)/shard_map/first/pallas_call | solution.py:536
  34.6 0.0 collective-permute-done.1
  34.6 0.0 slice-done
  34.6 0.2 slice-done.1
  34.8 3.2 %second.1 = (bf16[192,2048]{1,0:T(8,128)(2,1)S(1)}, bf16[384,512]{1,0:T(8,128)(2,1)S(1)}) custom-call(bf16[384,512]{1,0:T(8,128)(2,1)S(1)} %bitcast.15, f32[2,192,2048]{2,1,0:T(8,128)S(1)} %first.1.partial, bf16[2048,2048]{1,0:T(8,128)(2,1)S(1)} %copy-done, bf16[2048,2048]{1,0:T(8,128)(2,1)S(1)} %copy-done.1, bf16[2048,2048]{1,0:T(8,128)(2,1)S(1)} %bitcast.12), custom_call_target="tpu_custom_call" | custom-call | tf_op jit(solution)/shard_map/second/pallas_call | solution.py:548
  38.0 0.0 copy-start.2
  38.0 0.6 collective-permute-start.2
  38.6 1.4 %third.1 = bf16[384,512]{1,0:T(8,128)(2,1)S(1)} custom-call(bf16[192,2048]{1,0:T(8,128)(2,1)S(1)} %get-tuple-element.18.hidden, bf16[2048,2048]{1,0:T(8,128)(2,1)S(1)} %bitcast.12), custom_call_target="tpu_custom_call" | custom-call | flops 805306368 | bytes 4194304 | tf_op jit(solution)/shard_map/third/pallas_call | solution.py:557
  39.9 0.0 collective-permute-done.2
  39.9 0.1 add_convert_fusion
  40.0 16.5 %all_to_all.11 = bf16[16,24,512]{2,1,0:T(8,128)(2,1)S(1)} all-to-all(bf16[16,24,512]{2,1,0:T(8,128)(2,1)S(1)} %bitcast.18), channel_id=1, replica_groups=mesh['ep'=16,'tp'=2] {'ep'}, dimensions={0} | all-to-all | bytes 786432 | tf_op jit(solution)/shard_map/all_to_all | solution.py:570
  56.6 0.0 copy-done.2
  56.6 0.3 combine.1.half
  56.8 0.1 collective-permute-start.3
  56.9 1.2 %collective-permute-done.3.other = bf16[32,1024]{1,0:T(8,128)(2,1)S(1)} collective-permute-done((bf16[32,1024]{1,0:T(8,128)(2,1)S(1)}, bf16[32,1024]{1,0:T(8,128)(2,1)S(1)}, u32[]{:S(2)}, u32[]{:S(2)}) %collective-permute-start.3) | collective-permute-done | bytes 65568 | tf_op jit(solution)/shard_map/ppermute | solution.py:581
  58.2 0.7 %join.1 = bf16[32,2048]{1,0:T(8,128)(2,1)} custom-call(bf16[32,1024]{1,0:T(8,128)(2,1)S(1)} %combine.1.half, bf16[32,1024]{1,0:T(8,128)(2,1)S(1)} %collective-permute-done.3.other), custom_call_target="tpu_custom_call" | custom-call | tf_op jit(solution)/shard_map/join/pallas_call | solution.py:582
  (1 shorter events, 0.0 us)
Async XLA Ops:
  9.1 1.5 %collective-permute-start = (bf16[32,2048]{1,0:T(8,128)(2,1)S(1)}, bf16[32,2048]{1,0:T(8,128)(2,1)S(1)}, u32[]{:S(2)}, u32[]{:S(2)}) collective-permute-start(bf16[32,2048]{1,0:T(8,128)(2,1)S(1)} %get-tuple-element.14.own), channel_id=1, source_target_pairs={{0,1},{1,0},{2,3},{3,2},{4,5},{5,4},{6,7},{7,6},{8,9},{9,8},{10,11... | collective-permute-start | bytes 393224 | tf_op jit(solution)/shard_map/ppermute | solution.py:505
  10.6 22.0 %copy-start = (bf16[2048,2048]{1,0:T(8,128)(2,1)S(1)}, bf16[2048,2048]{1,0:T(8,128)(2,1)}, u32[]{:S(2)}) copy-start(bf16[2048,2048]{1,0:T(8,128)(2,1)} %w_gate.3) | copy-start | bytes 25165828
  10.6 22.0 %copy-start.1 = (bf16[2048,2048]{1,0:T(8,128)(2,1)S(1)}, bf16[2048,2048]{1,0:T(8,128)(2,1)}, u32[]{:S(2)}) copy-start(bf16[2048,2048]{1,0:T(8,128)(2,1)} %w_up.3) | copy-start | bytes 25165828
  11.1 23.6 %slice-start = ((s8[8388608]{0:T(1024)(128)(4,1)}), s8[4194304]{0:T(1024)(128)(4,1)S(1)}, s32[]{:S(2)}) async-start(s8[8388608]{0:T(1024)(128)(4,1)} %bitcast.11), calls=%async_computation.2 | async-start | bytes 8388608
  32.6 2.0 %collective-permute-start.1 = (bf16[16,24,512]{2,1,0:T(8,128)(2,1)S(1)}, bf16[16,24,512]{2,1,0:T(8,128)(2,1)S(1)}, u32[]{:S(2)}, u32[]{:S(2)}) collective-permute-start(bf16[16,24,512]{2,1,0:T(8,128)(2,1)S(1)} %all_to_all.10), channel_id=1, source_target_pairs={{0,1},{1,0},{2,3},{3,2},{4,5},{5,4},{6,7},{7,6},{8,9},{9,8},{10,11... | collective-permute-start | bytes 1179656 | tf_op jit(solution)/shard_map/ppermute | solution.py:529
  32.6 2.2 %slice-start.1 = ((s8[8388608]{0:T(1024)(128)(4,1)}), s8[4194304]{0:T(1024)(128)(4,1)S(1)}, s32[]{:S(2)}) async-start(s8[8388608]{0:T(1024)(128)(4,1)} %bitcast.11), calls=%async_computation.3 | async-start | bytes 8388608
  38.0 18.6 %copy-start.2 = (f32[32,2]{0,1:T(2,128)S(1)}, f32[32,2]{0,1:T(2,128)}, u32[]{:S(2)}) copy-start(f32[32,2]{0,1:T(2,128)} %param.30) | copy-start | bytes 772
  38.0 1.9 %collective-permute-start.2 = (bf16[384,512]{1,0:T(8,128)(2,1)S(1)}, bf16[384,512]{1,0:T(8,128)(2,1)S(1)}, u32[]{:S(2)}, u32[]{:S(2)}) collective-permute-start(bf16[384,512]{1,0:T(8,128)(2,1)S(1)} %get-tuple-element.19), channel_id=1, source_target_pairs={{0,1},{1,0},{2,3},{3,2},{4,5},{5,4},{6,7},{7,6},{8,9},{9,8},{10,11... | collective-permute-start | bytes 1179656 | tf_op jit(solution)/shard_map/ppermute | solution.py:568
  56.8 1.3 %collective-permute-start.3 = (bf16[32,1024]{1,0:T(8,128)(2,1)S(1)}, bf16[32,1024]{1,0:T(8,128)(2,1)S(1)}, u32[]{:S(2)}, u32[]{:S(2)}) collective-permute-start(bf16[32,1024]{1,0:T(8,128)(2,1)S(1)} %combine.1.half), channel_id=1, source_target_pairs={{0,1},{1,0},{2,3},{3,2},{4,5},{5,4},{6,7},{7,6},{8,9},{9,8},{10,11... | collective-permute-start | bytes 196616 | tf_op jit(solution)/shard_map/ppermute | solution.py:581

commit v3 on v2

--- a/solution.py
+++ b/solution.py
@@ -70,7 +70,7 @@
     count = row.shape[1]
     lane, sub = iota((count, count), 1), iota((count, count), 0)
     column = jnp.sum(jnp.where(lane == sub, row, 0), axis=1, keepdims=True)
-    before = (row > column) | ((row == column) & (lane < sub))
+    before = (row < column) | ((row == column) & (lane < sub))
     rank = jnp.sum(before.astype(f32), axis=1, keepdims=True)
     lane, sub = iota((count, LANES), 1), iota((count, LANES), 0)
     hit = rank == lane.astype(f32)
@@ -155,7 +155,7 @@
     )
 
     def chunks(g):
-        return (table_s[1, g * GROUP] + STEP - 1) // STEP
+        return (table_s[1, g * GROUP + GROUP - 1] + STEP - 1) // STEP
 
     def group_copies(g):
         window = pl.ds(STEP, pl.multiple_of((chunks(g) - 1) * STEP, STEP))
@@ -172,7 +172,7 @@
             )
         return pairs_of
 
-    for c in small + copies[:3] + [gate_copy, key_base, value_base, copies[3]]:
+    for c in small + copies[:3] + [gate_copy, key_base, value_base]:
         c.start()
     small[0].wait()
     order, length = sort_table(lengths_v[...])
@@ -193,6 +193,7 @@
         return 0
 
     lax.fori_loop(0, groups, start_group, 0)
+    copies[3].start()
 
     for c in small[1:]:
         c.wait()

time: 58.9 us -> 57.9 us (0.983)
  Pallas kernels: 16.9 us -> 15.7 us
    pallas_call x1, Pallas kernels: 9.09 us -> 7.82 us  [on_device(): pl.pallas_call(functools.partial(attention_kernel, pieces), name='attenti...]
where the time goes in v3:
time: 57.9 us; the launch traced here: 57.5 us
  blocking collectives  38 us (66%)
  Pallas kernels  15.7 us (27%)
  waiting for transfers between devices  2.23 us (4%)
  starting transfers between devices  1.2 us (2%)
    all_to_all x1, blocking collectives, on_device(): lax.all_to_all(outgoing.reshape(chips, 2 * CAP, quarter), 'ep', split_axi...  21.5 us
    all_to_all x1, blocking collectives, on_device(): lax.all_to_all(share.reshape(chips, 2 * CAP, quarter), 'ep', split_axis=0...  16.5 us
    pallas_call x1, Pallas kernels, on_device(): pl.pallas_call(functools.partial(attention_kernel, pieces), name='attenti...  7.82 us
    pallas_call x1, Pallas kernels, on_device(): pl.pallas_call(functools.partial(second_kernel, parts), name='second', ou...  3.18 us
    pallas_call x1, Pallas kernels, on_device(): pl.pallas_call(functools.partial(first_kernel, parts), name='first', cost...  1.99 us
    pallas_call x1, Pallas kernels, on_device(): pl.pallas_call(third_kernel, name='third', cost_estimate=pl.CostEstimate(...  1.35 us
    ppermute x1, waiting for transfers between devices, on_device(): other_half = lax.ppermute(half, 'tp', swap)  1.24 us
  transfers between devices with their start and end apart: 4, of which 2 were waited for; matrix products, arithmetic and copies ran while one was open for 0% of the time, Pallas kernels for 6%

profile of v3, /device:TPU:0, one launch (start us, length us, event | category | flops | bytes accessed | tf_op | source)
XLA Modules:
  0.0 57.5 jit_solution(8854523166121175502)
XLA Ops:
  0.0 7.8 %attention.1 = (bf16[32,2048]{1,0:T(8,128)(2,1)S(1)}, bf16[384,128]{1,0:T(8,128)(2,1)S(1)}, bf16[32,2048]{1,0:T(8,128)(2,1)S(1)}, f32[1,2048]{1,0:T(1,128)S(1)}) custom-call(s32[1,32]{1,0:T(1,128)} %bitcast.23, bf16[32,2048]{1,0:T(8,128)(2,1)} %tokens.1, f32[1,2048]{1,0:T(1,128)} %bitcast.20, f32[1,2048]{1,0:T(1,128)} %bitcast.21, bf16[8,2048]{1,0:T(8,128)(2,1)} %bitcast.19, ...), custom_call_target="tpu_custom_call" | custom-call | tf_op jit(solution)/shard_map/attention/pallas_call | solution.py:449
  7.8 0.6 collective-permute-start
  8.4 1.0 %collective-permute-done.other = bf16[32,2048]{1,0:T(8,128)(2,1)S(1)} collective-permute-done((bf16[32,2048]{1,0:T(8,128)(2,1)S(1)}, bf16[32,2048]{1,0:T(8,128)(2,1)S(1)}, u32[]{:S(2)}, u32[]{:S(2)}) %collective-permute-start) | collective-permute-done | bytes 131104 | tf_op jit(solution)/shard_map/ppermute | solution.py:506
  9.4 0.0 copy-start
  9.4 0.0 copy-start.1
  9.4 0.4 dispatch.1
  9.8 0.0 slice-start
  9.8 21.5 %all_to_all.10 = bf16[16,24,512]{2,1,0:T(8,128)(2,1)S(1)} all-to-all(bf16[16,24,512]{2,1,0:T(8,128)(2,1)S(1)} %bitcast.16), channel_id=1, replica_groups=mesh['ep'=16,'tp'=2] {'ep'}, dimensions={0} | all-to-all | bytes 786432 | tf_op jit(solution)/shard_map/all_to_all | solution.py:527
  31.3 0.0 collective-permute-start.1
  31.3 0.0 copy-done
  31.3 0.0 copy-done.1
  31.3 0.0 slice-start.1
  31.3 2.0 %first.1.partial = f32[2,192,2048]{2,1,0:T(8,128)S(1)} custom-call(bf16[384,512]{1,0:T(8,128)(2,1)S(1)} %bitcast.14, bf16[2048,2048]{1,0:T(8,128)(2,1)S(1)} %copy-done, bf16[2048,2048]{1,0:T(8,128)(2,1)S(1)} %copy-done.1), custom_call_target="tpu_custom_call" | custom-call | flops 1610612736 | bytes 8388608 | tf_op jit(solution)/shard_map/first/pallas_call | solution.py:537
  33.3 0.0 collective-permute-done.1
  33.3 0.0 slice-done
  33.3 0.2 slice-done.1
  33.5 3.2 %second.1 = (bf16[192,2048]{1,0:T(8,128)(2,1)S(1)}, bf16[384,512]{1,0:T(8,128)(2,1)S(1)}) custom-call(bf16[384,512]{1,0:T(8,128)(2,1)S(1)} %bitcast.15, f32[2,192,2048]{2,1,0:T(8,128)S(1)} %first.1.partial, bf16[2048,2048]{1,0:T(8,128)(2,1)S(1)} %copy-done, bf16[2048,2048]{1,0:T(8,128)(2,1)S(1)} %copy-done.1, bf16[2048,2048]{1,0:T(8,128)(2,1)S(1)} %bitcast.12), custom_call_target="tpu_custom_call" | custom-call | tf_op jit(solution)/shard_map/second/pallas_call | solution.py:549
  36.7 0.0 copy-start.2
  36.7 0.6 collective-permute-start.2
  37.3 1.4 %third.1 = bf16[384,512]{1,0:T(8,128)(2,1)S(1)} custom-call(bf16[192,2048]{1,0:T(8,128)(2,1)S(1)} %get-tuple-element.18.hidden, bf16[2048,2048]{1,0:T(8,128)(2,1)S(1)} %bitcast.12), custom_call_target="tpu_custom_call" | custom-call | flops 805306368 | bytes 4194304 | tf_op jit(solution)/shard_map/third/pallas_call | solution.py:558
  38.6 0.0 collective-permute-done.2
  38.6 0.1 add_convert_fusion
  38.8 16.5 %all_to_all.11 = bf16[16,24,512]{2,1,0:T(8,128)(2,1)S(1)} all-to-all(bf16[16,24,512]{2,1,0:T(8,128)(2,1)S(1)} %bitcast.18), channel_id=1, replica_groups=mesh['ep'=16,'tp'=2] {'ep'}, dimensions={0} | all-to-all | bytes 786432 | tf_op jit(solution)/shard_map/all_to_all | solution.py:571
  55.3 0.0 copy-done.2
  55.3 0.3 combine.1.half
  55.5 0.1 collective-permute-start.3
  55.6 1.2 %collective-permute-done.3.other = bf16[32,1024]{1,0:T(8,128)(2,1)S(1)} collective-permute-done((bf16[32,1024]{1,0:T(8,128)(2,1)S(1)}, bf16[32,1024]{1,0:T(8,128)(2,1)S(1)}, u32[]{:S(2)}, u32[]{:S(2)}) %collective-permute-start.3) | collective-permute-done | bytes 65568 | tf_op jit(solution)/shard_map/ppermute | solution.py:582
  56.9 0.7 %join.1 = bf16[32,2048]{1,0:T(8,128)(2,1)} custom-call(bf16[32,1024]{1,0:T(8,128)(2,1)S(1)} %combine.1.half, bf16[32,1024]{1,0:T(8,128)(2,1)S(1)} %collective-permute-done.3.other), custom_call_target="tpu_custom_call" | custom-call | tf_op jit(solution)/shard_map/join/pallas_call | solution.py:583
  (1 shorter events, 0.0 us)
Async XLA Ops:
  7.8 1.5 %collective-permute-start = (bf16[32,2048]{1,0:T(8,128)(2,1)S(1)}, bf16[32,2048]{1,0:T(8,128)(2,1)S(1)}, u32[]{:S(2)}, u32[]{:S(2)}) collective-permute-start(bf16[32,2048]{1,0:T(8,128)(2,1)S(1)} %get-tuple-element.14.own), channel_id=1, source_target_pairs={{0,1},{1,0},{2,3},{3,2},{4,5},{5,4},{6,7},{7,6},{8,9},{9,8},{10,11... | collective-permute-start | bytes 393224 | tf_op jit(solution)/shard_map/ppermute | solution.py:506
  9.4 21.9 %copy-start = (bf16[2048,2048]{1,0:T(8,128)(2,1)S(1)}, bf16[2048,2048]{1,0:T(8,128)(2,1)}, u32[]{:S(2)}) copy-start(bf16[2048,2048]{1,0:T(8,128)(2,1)} %w_gate.3) | copy-start | bytes 25165828
  9.4 21.9 %copy-start.1 = (bf16[2048,2048]{1,0:T(8,128)(2,1)S(1)}, bf16[2048,2048]{1,0:T(8,128)(2,1)}, u32[]{:S(2)}) copy-start(bf16[2048,2048]{1,0:T(8,128)(2,1)} %w_up.3) | copy-start | bytes 25165828
  9.8 23.5 %slice-start = ((s8[8388608]{0:T(1024)(128)(4,1)}), s8[4194304]{0:T(1024)(128)(4,1)S(1)}, s32[]{:S(2)}) async-start(s8[8388608]{0:T(1024)(128)(4,1)} %bitcast.11), calls=%async_computation.2 | async-start | bytes 8388608
  31.3 2.0 %collective-permute-start.1 = (bf16[16,24,512]{2,1,0:T(8,128)(2,1)S(1)}, bf16[16,24,512]{2,1,0:T(8,128)(2,1)S(1)}, u32[]{:S(2)}, u32[]{:S(2)}) collective-permute-start(bf16[16,24,512]{2,1,0:T(8,128)(2,1)S(1)} %all_to_all.10), channel_id=1, source_target_pairs={{0,1},{1,0},{2,3},{3,2},{4,5},{5,4},{6,7},{7,6},{8,9},{9,8},{10,11... | collective-permute-start | bytes 1179656 | tf_op jit(solution)/shard_map/ppermute | solution.py:530
  31.3 2.2 %slice-start.1 = ((s8[8388608]{0:T(1024)(128)(4,1)}), s8[4194304]{0:T(1024)(128)(4,1)S(1)}, s32[]{:S(2)}) async-start(s8[8388608]{0:T(1024)(128)(4,1)} %bitcast.11), calls=%async_computation.3 | async-start | bytes 8388608
  36.7 18.6 %copy-start.2 = (f32[32,2]{0,1:T(2,128)S(1)}, f32[32,2]{0,1:T(2,128)}, u32[]{:S(2)}) copy-start(f32[32,2]{0,1:T(2,128)} %param.30) | copy-start | bytes 772
  36.7 1.9 %collective-permute-start.2 = (bf16[384,512]{1,0:T(8,128)(2,1)S(1)}, bf16[384,512]{1,0:T(8,128)(2,1)S(1)}, u32[]{:S(2)}, u32[]{:S(2)}) collective-permute-start(bf16[384,512]{1,0:T(8,128)(2,1)S(1)} %get-tuple-element.19), channel_id=1, source_target_pairs={{0,1},{1,0},{2,3},{3,2},{4,5},{5,4},{6,7},{7,6},{8,9},{9,8},{10,11... | collective-permute-start | bytes 1179656 | tf_op jit(solution)/shard_map/ppermute | solution.py:569
  55.5 1.3 %collective-permute-start.3 = (bf16[32,1024]{1,0:T(8,128)(2,1)S(1)}, bf16[32,1024]{1,0:T(8,128)(2,1)S(1)}, u32[]{:S(2)}, u32[]{:S(2)}) collective-permute-start(bf16[32,1024]{1,0:T(8,128)(2,1)S(1)} %combine.1.half), channel_id=1, source_target_pairs={{0,1},{1,0},{2,3},{3,2},{4,5},{5,4},{6,7},{7,6},{8,9},{9,8},{10,11... | collective-permute-start | bytes 196616 | tf_op jit(solution)/shard_map/ppermute | solution.py:582
